TPU v7x, 256 devices: a 8x8x2 block of a 8x8x16 slice. The times are simulated.
256 devices in a mesh: grp: 2 (over z), ep: 64 (over y, x), tp: 2 (over core).
Axes of the slice: x: 8, y: 8, z: 2, core: 2. Of those that a mesh axis runs over, the one named last changes fastest.
The devices are a block of a 8x8x16 slice.
Arguments:
- tokens_in: bfloat16 [8192, 2048], P(('grp', 'ep')), parts along dimension 0, may hold values from -6 to 6
- norm_gain: float32 [2048], replicated, may hold values from 0.1 to 1.9
- gate_proj: bfloat16 [64, 2048, 1024], P('ep', None, 'tp'), may hold values from -0.125 to 0.125
- up_proj: bfloat16 [64, 2048, 1024], P('ep', None, 'tp'), may hold values from -0.125 to 0.125
- down_proj: bfloat16 [64, 1024, 2048], P('ep', 'tp'), may hold values from -0.1875 to 0.1875
- route_ids: int32 [8192, 8], P(('grp', 'ep')), parts along dimension 0, may hold values from 0 to 63, all different within a row; in each aligned block of 64 rows (0 to 63, 64 to 127, ...) at most 16 rows name the same one
- group_weight: float32 [8192, 8], P(('grp', 'ep')), parts along dimension 0, may hold values from 0.05 to 1
- expert_weight: float32 [8192, 8], P(('grp', 'ep')), parts along dimension 0, may hold values from 0.05 to 1
Outputs:
- expert_mix: bfloat16 [8192, 2048], P(('grp', 'ep'), 'tp'), parts along dimension 0
There are 2 independent parts, one for each index of `grp`. A program takes and returns all parts, laid end to end along the dimension named above; an argument that names none is the same for every part. Nothing has to cross between parts.
Inputs may be any that keep to these rules, and one draw needn't show every extreme that they name: `route_ids`: each row names 8 different experts; within the rows of one index of ep no expert is named by more than 16 rows, a bound that some of them reach.
All inputs are finite; a program needn't handle non-finite values.
Results may differ from a plain program's by a relative error of at most 0.0077.
Values may be sent and summed in bfloat16 or wider, within the bound.
No kernel may reach another device: no remote copies, remote signals or barrier semaphores. Data moves between devices by JAX's collectives and lax.ppermute only.
A program may use at most 64 MiB of HBM per device.

v0:
```python
import jax
import jax.numpy as jnp
from jax import lax
from jax.sharding import PartitionSpec as P

TOP = 8
EXP_GRP = 8


EPSILON = 1e-06


def cut_along(array, dim, size):
    lengths = array.shape
    blocks = array.reshape(*lengths[:dim], size, lengths[dim] // size, *lengths[dim + 1 :])
    return jnp.moveaxis(blocks, dim, 0)


def sum_at_owner(array, axis, dim):
    size = lax.axis_size(axis)
    blocks = lax.all_to_all(cut_along(array, dim, size), axis, 0, 0, tiled=True)
    return jnp.sum(blocks.astype(jnp.float32), axis=0)


def on_device(
    tokens_in, norm_gain, gate_proj, up_proj, down_proj, route_ids, group_weight, expert_weight
):
    token_count, model_width = tokens_in.shape
    expert_count = gate_proj.shape[0] * lax.axis_size("ep")
    lane_count = lax.axis_size("tp")
    part_width = model_width // lane_count
    capacity = min(token_count, max(2, 2 * token_count * TOP // expert_count))
    slot_total = expert_count * capacity
    row_values = tokens_in.astype(jnp.float32)
    inv_scale = lax.rsqrt(jnp.mean(row_values * row_values, axis=-1, keepdims=True) + EPSILON)
    normed = (row_values * inv_scale * norm_gain).astype(jnp.bfloat16)
    route_count = token_count * TOP
    flat_ids = route_ids.reshape(route_count)
    positions = jnp.arange(route_count, dtype=jnp.int32)
    same_expert = (flat_ids[:, None] == flat_ids[None, :]) & (
        positions[None, :] < positions[:, None]
    )
    slot_rank = jnp.sum(same_expert.astype(jnp.int32), axis=1)
    slot_index = flat_ids * capacity + slot_rank
    slot_match = jnp.arange(slot_total, dtype=jnp.int32)[:, None] == slot_index[None, :]
    selector = jnp.sum(
        slot_match.reshape(slot_total, token_count, TOP).astype(jnp.int32), axis=2
    ).astype(jnp.bfloat16)
    gate_local = gate_proj[0]
    up_local = up_proj[0]
    lane_index = lax.axis_index("tp")
    own_half = lax.dynamic_slice_in_dim(normed, lane_index * part_width, part_width, 1)
    outgoing = jnp.dot(selector, own_half, preferred_element_type=jnp.float32).astype(jnp.bfloat16)
    arrived = lax.all_to_all(
        outgoing.reshape(expert_count, capacity, part_width),
        "ep",
        split_axis=0,
        concat_axis=0,
        tiled=True,
    )
    arrived = arrived.reshape(slot_total, part_width)
    column_piece = lax.all_gather(arrived, "tp", axis=1, tiled=True)
    gate_acts = jnp.dot(column_piece, gate_local, preferred_element_type=jnp.float32)
    up_acts = jnp.dot(column_piece, up_local, preferred_element_type=jnp.float32)
    hidden = (jax.nn.silu(gate_acts) * up_acts).astype(jnp.bfloat16)
    partial_rows = jnp.dot(hidden, down_proj[0], preferred_element_type=jnp.float32)
    summed = sum_at_owner(
        partial_rows.reshape(expert_count, capacity, model_width).astype(jnp.bfloat16), "tp", 2
    )
    results = summed.astype(jnp.bfloat16)
    returned = lax.all_to_all(results, "ep", split_axis=0, concat_axis=0, tiled=True).reshape(
        slot_total, part_width
    )
    picked = returned[slot_index].astype(jnp.float32).reshape(token_count, TOP, part_width)
    group_ids = route_ids // EXP_GRP
    group_count = group_weight.shape[1]
    group_match = (
        group_ids[:, :, None] == jnp.arange(group_count, dtype=jnp.int32)[None, None, :]
    ).astype(jnp.float32)
    group_part = jnp.sum(group_weight[:, None, :] * group_match, axis=2)
    gate_values = group_part * expert_weight / jnp.sum(expert_weight, axis=1, keepdims=True)
    return jnp.sum(picked * gate_values[:, :, None], axis=1).astype(jnp.bfloat16)


def solution(mesh):
    in_specs = (
        P(("grp", "ep"), None),
        P(),
        P("ep", None, "tp"),
        P("ep", None, "tp"),
        P("ep", "tp", None),
        P(("grp", "ep"), None),
        P(("grp", "ep"), None),
        P(("grp", "ep"), None),
    )
    out_specs = P(("grp", "ep"), "tp")
    return jax.shard_map(
        on_device, mesh=mesh, in_specs=in_specs, out_specs=out_specs, check_vma=False
    )
```

profile of v0, /device:TPU:514, one launch (start us, length us, event | category | flops | bytes accessed | tf_op | source)
XLA Modules:
  0.0 216.0 jit_solution(7506265072580166607)
XLA Ops:
  6.6 1.1 convert_element_type.40
  7.7 1.1 multiply_reduce_fusion
  8.8 0.8 copy.24
  9.6 0.1 eq.43
  9.7 0.3 convert_reduce_fusion.1
  9.9 0.1 reduce_sum.71
  10.0 0.7 convert_reduce_fusion
  10.7 0.7 dynamic-slice
  11.4 0.8 convolution_convert_fusion.1
  12.2 72.0 %all_to_all.15 = bf16[64,16,1024]{2,1,0:T(8,128)(2,1)} all-to-all(bf16[64,16,1024]{2,1,0:T(8,128)(2,1)S(1)} %bitcast.33), channel_id=1, replica_groups=mesh['grp'=2,'ep'=64,'tp'=2] {'ep'}, dimensions={0} | all-to-all | bytes 4194304 | tf_op jit(solution)/shard_map/all_to_all | solution.py:54
  84.2 0.1 all-gather.2.cloned.1.call-update
  84.2 28.4 %all-gather.2.cloned.1.call-done = bf16[1024,2048]{1,0:T(8,128)(2,1)} async-done(((bf16[1024,1024]{1,0:T(8,128)(2,1)}), bf16[1024,2048]{1,0:T(8,128)(2,1)}) %all-gather.2.cloned.1.call-update) | async-done | bytes 4194320 | tf_op jit(solution)/shard_map/all_gather | solution.py:62
  112.7 5.3 %fusion.2 = f32[1024,512]{1,0:T(8,128)S(1)} fusion(bf16[1024,2048]{1,0:T(8,128)(2,1)} %all-gather.2.cloned.1.call-done, bf16[1,2048,512]{2,1,0:T(8,128)(2,1)} %param.11), kind=kOutput, calls=%fused_computation.6 | convolution fusion | flops 2147483648 | bytes 8388608 | tf_op jit(solution)/shard_map/dot_general | solution.py:64
  118.0 2.6 %multiply_convert_fusion = bf16[1024,512]{1,0:T(8,128)(2,1)S(1)} fusion(f32[1024,512]{1,0:T(8,128)S(1)} %fusion.2, bf16[1024,2048]{1,0:T(8,128)(2,1)S(1)} %copy-done.4, bf16[1,2048,512]{2,1,0:T(8,128)(2,1)S(1)} %copy-done.5), kind=kOutput, calls=%fused_computation.10 | convolution fusion | flops 2150629376 | bytes 9437184 | tf_op jit(solution)/shard_map/dot_general | solution.py:63
  120.7 2.3 %convolution_convert_fusion = bf16[64,16,2048]{2,1,0:T(8,128)(2,1)S(1)} fusion(bf16[64,16,512]{2,1,0:T(8,128)(2,1)S(1)} %bitcast.37, bf16[1,512,2048]{2,1,0:T(8,128)(2,1)S(1)} %copy-done), kind=kOutput, calls=%fused_computation.2 | convolution fusion | flops 2149580800 | bytes 7340032 | tf_op jit(solution)/shard_map/dot_general | solution.py:66
  123.0 0.6 copy.30
  123.7 8.2 %all_to_all.16 = bf16[2,64,16,1024]{3,2,1,0:T(8,128)(2,1)} all-to-all(bf16[2,64,16,1024]{3,2,1,0:T(8,128)(2,1)S(1)} %bitcast.31), channel_id=1, replica_groups=mesh['grp'=2,'ep'=64,'tp'=2] {'tp'}, dimensions={0} | all-to-all | bytes 8388608 | tf_op jit(solution)/shard_map/all_to_all | solution.py:21
  131.8 5.2 %reduce_sum.74 = bf16[64,16,1024]{2,1,0:T(8,128)(2,1)} reduce(bf16[2,64,16,1024]{3,2,1,0:T(8,128)(2,1)} %all_to_all.16, bf16[]{:T(256)} %constant.37.clone.1), dimensions={0}, to_apply=%region_3.4 | reduce | flops 1048576 | bytes 6291458 | tf_op jit(solution)/shard_map/reduce_sum | solution.py:22
  137.1 13.9 %all-to-all-start.2 = ((bf16[64,16,1024]{2,1,0:T(8,128)(2,1)}), bf16[64,16,1024]{2,1,0:T(8,128)(2,1)}, u32[]{:S(2)}, u32[]{:S(2)}) async-start(bf16[64,16,1024]{2,1,0:T(8,128)(2,1)} %reduce_sum.74), calls=%async_computation.2 | async-start | bytes 4194304 | tf_op jit(solution)/shard_map/all_to_all | solution.py:71
  150.9 0.1 mul.78
  151.1 0.1 copy.27
  151.2 51.9 %all-to-all-done.2 = bf16[64,16,1024]{2,1,0:T(8,128)(2,1)} async-done(((bf16[64,16,1024]{2,1,0:T(8,128)(2,1)}), bf16[64,16,1024]{2,1,0:T(8,128)(2,1)}, u32[]{:S(2)}, u32[]{:S(2)}) %all-to-all-start.2) | async-done | bytes 2097184 | tf_op jit(solution)/shard_map/all_to_all | solution.py:71
  203.2 4.6 %gather_fusion = bf16[512,1024]{1,0:T(8,128)(2,1)S(1)} fusion(bf16[1024,1024]{1,0:T(8,128)(2,1)} %bitcast.8, s32[1024]{0:T(1024)S(1)} %pad_clamp_fusion), kind=kCustom, calls=%fused_computation | custom fusion | bytes 2099200 | tf_op jit(solution)/shard_map/gather | solution.py:74
  207.8 1.4 fusion
  (21 shorter events, 0.1 us)
Async XLA Ops:
  6.5 114.1 %copy-start = (bf16[1,512,2048]{2,1,0:T(8,128)(2,1)S(1)}, bf16[1,512,2048]{2,1,0:T(8,128)(2,1)}, u32[]{:S(2)}) copy-start(bf16[1,512,2048]{2,1,0:T(8,128)(2,1)} %param.12) | copy-start | bytes 6291460
  6.6 106.1 %all-gather.2.cloned.1.call-start = ((), (), s32[]{:S(2)}) async-start(), calls=%async_computation.3 | async-start | bytes 6291456 | tf_op jit(solution)/shard_map/all_gather | solution.py:62
  112.6 5.3 %copy-start.4 = (bf16[1024,2048]{1,0:T(8,128)(2,1)S(1)}, bf16[1024,2048]{1,0:T(8,128)(2,1)}, u32[]{:S(2)}) copy-start(bf16[1024,2048]{1,0:T(8,128)(2,1)} %all-gather.2.cloned.1.call-done) | copy-start | bytes 12582916
  112.6 5.3 %copy-start.5 = (bf16[1,2048,512]{2,1,0:T(8,128)(2,1)S(1)}, bf16[1,2048,512]{2,1,0:T(8,128)(2,1)}, u32[]{:S(2)}) copy-start(bf16[1,2048,512]{2,1,0:T(8,128)(2,1)} %param.10) | copy-start | bytes 6291460
  137.1 14.0 %copy-start.1 = (f32[64,8]{0,1:T(8,128)S(1)}, f32[64,8]{0,1:T(8,128)}, u32[]{:S(2)}) copy-start(f32[64,8]{0,1:T(8,128)} %param.15) | copy-start | bytes 6148
  137.1 14.0 %copy-start.2 = (s32[64,8]{0,1:T(8,128)S(1)}, s32[64,8]{0,1:T(8,128)}, u32[]{:S(2)}) copy-start(s32[64,8]{0,1:T(8,128)} %param.13) | copy-start | bytes 6148
  137.1 14.0 %copy-start.3 = (f32[64,8]{0,1:T(8,128)S(1)}, f32[64,8]{0,1:T(8,128)}, u32[]{:S(2)}) copy-start(f32[64,8]{0,1:T(8,128)} %param.14) | copy-start | bytes 6148
  137.1 66.1 %all-to-all-start.2 = ((bf16[64,16,1024]{2,1,0:T(8,128)(2,1)}), bf16[64,16,1024]{2,1,0:T(8,128)(2,1)}, u32[]{:S(2)}, u32[]{:S(2)}) async-start(bf16[64,16,1024]{2,1,0:T(8,128)(2,1)} %reduce_sum.74), calls=%async_computation.2 | async-start | bytes 4194304 | tf_op jit(solution)/shard_map/all_to_all | solution.py:71
Sparse Core Ops, SparseCore 0:
  84.4 28.2 all-gather.1
where the time goes:
time: 216 us
  waiting for transfers between devices  80.4 us (37%)
  blocking collectives  80.2 us (37%)
  starting transfers between devices  13.9 us (6%)
  between operations  13.6 us (6%)
  matrix products  11.1 us (5%)
  other arithmetic  9.82 us (5%)
  local copies, waits for them, and re-layouts  7.08 us (3%)
    all_to_all x1, blocking collectives, on_device(): lax.all_to_all(outgoing.reshape(expert_count, capacity, part_width), 'ep'...  72 us
    all_to_all x1, waiting for transfers between devices, on_device(): lax.all_to_all(results, 'ep', split_axis=0, concat_axis=0, tiled=True)  51.9 us
    all_gather x1, waiting for transfers between devices, on_device(): column_piece = lax.all_gather(arrived, 'tp', axis=1, tiled=True)  28.4 us
    all_to_all x1, starting transfers between devices, on_device(): lax.all_to_all(results, 'ep', split_axis=0, concat_axis=0, tiled=True)  13.9 us
    all_to_all x1, blocking collectives, sum_at_owner(): blocks = lax.all_to_all(cut_along(array, dim, size), axis, 0, 0, tiled=True)  8.19 us
    dot_general x1, matrix products, on_device(): jnp.dot(column_piece, up_local, preferred_element_type=jnp.float32)  5.32 us
    reduce_sum x1, other arithmetic, sum_at_owner(): return jnp.sum(blocks.astype(jnp.float32), axis=0)  5.22 us
    gather x1, local copies, waits for them, and re-layouts, on_device(): returned[slot_index].astype(jnp.float32)  4.59 us
  transfers between devices with their start and end apart: 2, of which 2 were waited for; matrix products, arithmetic and copies ran while one was open for 0% of the time, Pallas kernels for 0%

commit v1 on v0

--- a/solution.py
+++ b/solution.py
@@ -59,7 +59,13 @@
         tiled=True,
     )
     arrived = arrived.reshape(slot_total, part_width)
-    column_piece = lax.all_gather(arrived, "tp", axis=1, tiled=True)
+    swap = [(lane, lane_count - 1 - lane) for lane in range(lane_count)]
+    partner = lax.ppermute(arrived, "tp", swap)
+    column_piece = jnp.where(
+        lane_index == 0,
+        jnp.concatenate([arrived, partner], axis=1),
+        jnp.concatenate([partner, arrived], axis=1),
+    )
     gate_acts = jnp.dot(column_piece, gate_local, preferred_element_type=jnp.float32)
     up_acts = jnp.dot(column_piece, up_local, preferred_element_type=jnp.float32)
     hidden = (jax.nn.silu(gate_acts) * up_acts).astype(jnp.bfloat16)

time: 216 us -> 180 us (0.83)
  waiting for transfers between devices: 80.4 us -> 56.5 us
  between operations: 13.6 us -> 0.17 us
  starting transfers between devices: 13.9 us -> 9.25 us
  matrix products: 11.1 us -> 15.1 us
    all_gather x1 -> x0, waiting for transfers between devices: 28.4 us -> none  [on_device(): column_piece = lax.all_gather(arrived, 'tp', axis=1, tiled=True)]
    all_to_all x1, starting transfers between devices: 13.9 us -> 9.24 us  [on_device(): lax.all_to_all(results, 'ep', split_axis=0, concat_axis=0, tiled=True)]
    ppermute x0 -> x1, waiting for transfers between devices: none -> 4.5 us  [on_device(): partner = lax.ppermute(arrived, 'tp', swap)]
    dot_general x1, matrix products: 2.64 us -> 6 us  [on_device(): jnp.dot(column_piece, gate_local, preferred_element_type=jnp.float32)]
where the time goes in v1:
time: 180 us; the launch traced here: 178 us
  blocking collectives  80.2 us (45%)
  waiting for transfers between devices  56.5 us (31%)
  matrix products  15.1 us (8%)
  other arithmetic  9.84 us (5%)
  starting transfers between devices  9.25 us (5%)
  local copies, waits for them, and re-layouts  7.07 us (4%)
    all_to_all x1, blocking collectives, on_device(): lax.all_to_all(outgoing.reshape(expert_count, capacity, part_width), 'ep'...  72 us
    all_to_all x1, waiting for transfers between devices, on_device(): lax.all_to_all(results, 'ep', split_axis=0, concat_axis=0, tiled=True)  52 us
    all_to_all x1, starting transfers between devices, on_device(): lax.all_to_all(results, 'ep', split_axis=0, concat_axis=0, tiled=True)  9.24 us
    all_to_all x1, blocking collectives, sum_at_owner(): blocks = lax.all_to_all(cut_along(array, dim, size), axis, 0, 0, tiled=True)  8.19 us
    dot_general x1, matrix products, on_device(): jnp.dot(column_piece, up_local, preferred_element_type=jnp.float32)  6.05 us
    dot_general x1, matrix products, on_device(): jnp.dot(column_piece, gate_local, preferred_element_type=jnp.float32)  6 us
    reduce_sum x1, other arithmetic, sum_at_owner(): return jnp.sum(blocks.astype(jnp.float32), axis=0)  5.22 us
    gather x1, local copies, waits for them, and re-layouts, on_device(): returned[slot_index].astype(jnp.float32)  4.59 us
  transfers between devices with their start and end apart: 2, of which 2 were waited for; matrix products, arithmetic and copies ran while one was open for 0% of the time, Pallas kernels for 0%

profile of v1, /device:TPU:514, one launch (start us, length us, event | category | flops | bytes accessed | tf_op | source)
XLA Modules:
  0.0 178.2 jit_solution(1446008462244357383)
XLA Ops:
  0.0 1.1 convert_element_type.40
  1.1 1.1 multiply_reduce_fusion
  2.3 0.8 copy.24
  3.0 0.1 eq.47
  3.1 0.3 convert_reduce_fusion.1
  3.4 0.1 reduce_sum.71
  3.5 0.7 convert_reduce_fusion
  4.2 0.7 dynamic-slice
  4.9 0.8 convolution_convert_fusion.1
  5.6 72.0 %all_to_all.15 = bf16[64,16,1024]{2,1,0:T(8,128)(2,1)} all-to-all(bf16[64,16,1024]{2,1,0:T(8,128)(2,1)S(1)} %bitcast.30), channel_id=1, replica_groups=mesh['grp'=2,'ep'=64,'tp'=2] {'ep'}, dimensions={0} | all-to-all | bytes 4194304 | tf_op jit(solution)/shard_map/all_to_all | solution.py:54
  77.6 0.0 collective-permute-start
  77.6 4.5 %collective-permute-done = bf16[1024,1024]{1,0:T(8,128)(2,1)} collective-permute-done((bf16[1024,1024]{1,0:T(8,128)(2,1)}, bf16[1024,1024]{1,0:T(8,128)(2,1)}, u32[]{:S(2)}, u32[]{:S(2)}) %collective-permute-start) | collective-permute-done | bytes 2097184 | tf_op jit(solution)/shard_map/ppermute | solution.py:63
  82.1 6.0 %fusion.4 = f32[1024,512]{1,0:T(8,128)S(1)} fusion(bf16[1,2048,512]{2,1,0:T(8,128)(2,1)} %param.10, bf16[1024,1024]{1,0:T(8,128)(2,1)} %collective-permute-done, bf16[1024,1024]{1,0:T(8,128)(2,1)} %bitcast.1, pred[]{:T(512)S(6)} %eq.45), kind=kOutput, calls=%fused_computation.9 | convolution fusion | flops 2166358016 | bytes 8388609 | tf_op jit(solution)/shard_map/dot_general | solution.py:69
  88.1 6.1 %multiply_convert_fusion = bf16[1024,512]{1,0:T(8,128)(2,1)S(1)} fusion(f32[1024,512]{1,0:T(8,128)S(1)} %fusion.4, bf16[1,2048,512]{2,1,0:T(8,128)(2,1)S(1)} %copy-done.4, bf16[1024,1024]{1,0:T(8,128)(2,1)} %collective-permute-done, bf16[1024,1024]{1,0:T(8,128)(2,1)} %bitcast.1, pred[]{:T(512)S(6)} %eq.45), kind=kOutput, calls=%fused_computation.11 | convolution fusion | flops 2169503744 | bytes 9437185 | tf_op jit(solution)/shard_map/dot_general | solution.py:70
  94.2 2.3 %convolution_convert_fusion = bf16[64,16,2048]{2,1,0:T(8,128)(2,1)S(1)} fusion(bf16[64,16,512]{2,1,0:T(8,128)(2,1)S(1)} %bitcast.34, bf16[1,512,2048]{2,1,0:T(8,128)(2,1)S(1)} %copy-done), kind=kOutput, calls=%fused_computation.3 | convolution fusion | flops 2149580800 | bytes 7340032 | tf_op jit(solution)/shard_map/dot_general | solution.py:72
  96.6 0.6 copy.30
  97.2 8.2 %all_to_all.16 = bf16[2,64,16,1024]{3,2,1,0:T(8,128)(2,1)} all-to-all(bf16[2,64,16,1024]{3,2,1,0:T(8,128)(2,1)S(1)} %bitcast.29), channel_id=1, replica_groups=mesh['grp'=2,'ep'=64,'tp'=2] {'tp'}, dimensions={0} | all-to-all | bytes 8388608 | tf_op jit(solution)/shard_map/all_to_all | solution.py:21
  105.4 5.2 %reduce_sum.74 = bf16[64,16,1024]{2,1,0:T(8,128)(2,1)} reduce(bf16[2,64,16,1024]{3,2,1,0:T(8,128)(2,1)} %all_to_all.16, bf16[]{:T(256)} %constant.37.clone.1), dimensions={0}, to_apply=%region_3.4 | reduce | flops 1048576 | bytes 6291458 | tf_op jit(solution)/shard_map/reduce_sum | solution.py:22
  110.6 9.2 %all-to-all-start.2 = ((bf16[64,16,1024]{2,1,0:T(8,128)(2,1)}), bf16[64,16,1024]{2,1,0:T(8,128)(2,1)}, u32[]{:S(2)}, u32[]{:S(2)}) async-start(bf16[64,16,1024]{2,1,0:T(8,128)(2,1)} %reduce_sum.74), calls=%async_computation.2 | async-start | bytes 4194304 | tf_op jit(solution)/shard_map/all_to_all | solution.py:77
  119.9 0.1 mul.78
  120.1 0.1 copy.27
  120.2 52.0 %all-to-all-done.2 = bf16[64,16,1024]{2,1,0:T(8,128)(2,1)} async-done(((bf16[64,16,1024]{2,1,0:T(8,128)(2,1)}), bf16[64,16,1024]{2,1,0:T(8,128)(2,1)}, u32[]{:S(2)}, u32[]{:S(2)}) %all-to-all-start.2) | async-done | bytes 2097184 | tf_op jit(solution)/shard_map/all_to_all | solution.py:77
  172.2 4.6 %gather_fusion = bf16[512,1024]{1,0:T(8,128)(2,1)S(1)} fusion(bf16[1024,1024]{1,0:T(8,128)(2,1)} %bitcast.8, s32[1024]{0:T(1024)S(1)} %pad_clamp_fusion), kind=kCustom, calls=%fused_computation | custom fusion | bytes 2099200 | tf_op jit(solution)/shard_map/gather | solution.py:80
  176.8 1.4 fusion
  (18 shorter events, 0.1 us)
Async XLA Ops:
  0.0 94.2 %copy-start = (bf16[1,512,2048]{2,1,0:T(8,128)(2,1)S(1)}, bf16[1,512,2048]{2,1,0:T(8,128)(2,1)}, u32[]{:S(2)}) copy-start(bf16[1,512,2048]{2,1,0:T(8,128)(2,1)} %param.12) | copy-start | bytes 6291460
  77.6 4.5 %collective-permute-start = (bf16[1024,1024]{1,0:T(8,128)(2,1)}, bf16[1024,1024]{1,0:T(8,128)(2,1)}, u32[]{:S(2)}, u32[]{:S(2)}) collective-permute-start(bf16[1024,1024]{1,0:T(8,128)(2,1)} %bitcast.1), channel_id=1, source_target_pairs={{0,1},{1,0},{2,3},{3,2},{4,5},{5,4},{6,7},{7,6},{8,9},{9,8},{10,11... | collective-permute-start | bytes 6291464 | tf_op jit(solution)/shard_map/ppermute | solution.py:63
  77.6 10.5 %copy-start.4 = (bf16[1,2048,512]{2,1,0:T(8,128)(2,1)S(1)}, bf16[1,2048,512]{2,1,0:T(8,128)(2,1)}, u32[]{:S(2)}) copy-start(bf16[1,2048,512]{2,1,0:T(8,128)(2,1)} %param.11) | copy-start | bytes 6291460
  110.6 9.4 %copy-start.1 = (f32[64,8]{0,1:T(8,128)S(1)}, f32[64,8]{0,1:T(8,128)}, u32[]{:S(2)}) copy-start(f32[64,8]{0,1:T(8,128)} %param.15) | copy-start | bytes 6148
  110.6 9.4 %copy-start.2 = (s32[64,8]{0,1:T(8,128)S(1)}, s32[64,8]{0,1:T(8,128)}, u32[]{:S(2)}) copy-start(s32[64,8]{0,1:T(8,128)} %param.13) | copy-start | bytes 6148
  110.6 9.4 %copy-start.3 = (f32[64,8]{0,1:T(8,128)S(1)}, f32[64,8]{0,1:T(8,128)}, u32[]{:S(2)}) copy-start(f32[64,8]{0,1:T(8,128)} %param.14) | copy-start | bytes 6148
  110.6 61.6 %all-to-all-start.2 = ((bf16[64,16,1024]{2,1,0:T(8,128)(2,1)}), bf16[64,16,1024]{2,1,0:T(8,128)(2,1)}, u32[]{:S(2)}, u32[]{:S(2)}) async-start(bf16[64,16,1024]{2,1,0:T(8,128)(2,1)} %reduce_sum.74), calls=%async_computation.2 | async-start | bytes 4194304 | tf_op jit(solution)/shard_map/all_to_all | solution.py:77

commit v2 on v0

v2 whole, which is shorter than its diff:
```python
import functools

import jax
import jax.numpy as jnp
from jax import lax
from jax.experimental import pallas as pl
from jax.experimental.pallas import tpu as pltpu
from jax.sharding import PartitionSpec as P


TOP = 8
EXP_GRP = 8
LANES = 128

EPSILON = 1e-06
AXES = ("ep", "tp")


def shift_pairs(gathering, delta):
    lanes = lax.axis_size("tp")
    side = EXP_GRP
    pairs = []
    for device in range(lax.axis_size("ep")):
        row, col = divmod(device, side)
        for lane in range(lanes):
            if (lane == 0) == gathering:
                target = ((row + delta) % side) * side + col
            else:
                target = row * side + (col + delta) % side
            pairs.append((device * lanes + lane, target * lanes + lane))
    return pairs


def shift(array, gathering, delta):
    return lax.ppermute(array, AXES, shift_pairs(gathering, delta))


def call(kernel, outputs, *operands, scalars=0, scratch=(), far=False, limit=8):
    smem = pl.BlockSpec(memory_space=pltpu.SMEM)
    vmem = pl.BlockSpec(memory_space=pltpu.VMEM)
    rest = pl.BlockSpec(memory_space=pltpu.HBM) if far else vmem
    return pl.pallas_call(
        kernel,
        out_shape=[jax.ShapeDtypeStruct(*output) for output in outputs],
        in_specs=[smem] * scalars + [rest] * (len(operands) - scalars),
        out_specs=[vmem] * len(outputs),
        scratch_shapes=list(scratch),
        compiler_params=pltpu.CompilerParams(vmem_limit_bytes=limit << 20),
    )(*operands)


def fdot(left, right, contract=((1,), (0,))):
    return lax.dot_general(left, right, (contract, ((), ())), preferred_element_type=jnp.float32)


def prepare_kernel(lane_ref, *refs):
    far, out_ref, near, sems = refs[:5], refs[5], refs[6:11], refs[11]
    copies = [pltpu.make_async_copy(far[n], near[n], sems.at[n]) for n in range(5)]
    for copy in copies:
        copy.start()
    for copy in copies:
        copy.wait()
    tokens_ref, gain_ref, ids_ref, group_ref, expert_ref = near
    half = out_ref.shape[1] - LANES
    width = tokens_ref.shape[1]
    values = tokens_ref[...].astype(jnp.float32)
    mean = jnp.sum(values * values, axis=1, keepdims=True) / width
    scale = lax.rsqrt(mean + EPSILON)
    start = pl.multiple_of(lane_ref[0] * half, half)
    own = tokens_ref[:, pl.ds(start, half)].astype(jnp.float32)
    out_ref[:, :half] = (own * scale * gain_ref[:, pl.ds(start, half)]).astype(jnp.bfloat16)
    ids = ids_ref[...]
    group_ids = lax.div(ids, jnp.full_like(ids, EXP_GRP))
    part = jnp.zeros(ids.shape, jnp.float32)
    for group in range(group_ref.shape[0]):
        part += jnp.where(group_ids == group, group_ref[group : group + 1, :], 0.0)
    weights = expert_ref[...]
    gates = part * weights / jnp.sum(weights, axis=0, keepdims=True)
    high = gates.astype(jnp.bfloat16)
    rest = gates - high.astype(jnp.float32)
    middle = rest.astype(jnp.bfloat16)
    lowest = (rest - middle.astype(jnp.float32)).astype(jnp.bfloat16)
    place = lax.broadcasted_iota(jnp.int32, (TOP, LANES), 0)
    column = lax.broadcasted_iota(jnp.int32, (TOP, LANES), 1)
    packed = jnp.zeros((out_ref.shape[0], LANES), jnp.float32)
    terms = (ids.astype(jnp.float32).astype(jnp.bfloat16), high, middle, lowest)
    for number, term in enumerate(terms):
        spot = (column == place + number * TOP).astype(jnp.float32).astype(jnp.bfloat16)
        packed += fdot(term, spot, ((0,), (0,)))
    out_ref[:, half:] = packed.astype(jnp.bfloat16)


def select_kernel(capacity, targets_ref, *refs):
    side = EXP_GRP
    blocks, outs, factors_ref, held = refs[:side], refs[side : 2 * side], refs[2 * side], refs[-1]
    tokens = blocks[0].shape[0]
    half = outs[0].shape[1]
    for source in range(side):
        held[source] = blocks[source][...]
    lane = lax.broadcasted_iota(jnp.int32, (1, LANES), 1)
    target = jnp.zeros((1, LANES), jnp.int32)
    for number in range(side):
        target = jnp.where(lane // capacity == number, targets_ref[number], target)
    target = target.astype(jnp.float32)
    slot = (lane % capacity).astype(jnp.float32)
    below = lax.broadcasted_iota(jnp.int32, (tokens, tokens), 0)
    above = lax.broadcasted_iota(jnp.int32, (tokens, tokens), 1)
    before = (above < below).astype(jnp.float32).astype(jnp.bfloat16)

    def one_source(source, carry):
        info = held[source, :, half:].astype(jnp.float32)
        gates = (
            info
            + pltpu.roll(info, LANES - TOP, 1)
            + pltpu.roll(info, LANES - 2 * TOP, 1)
        )
        named = jnp.zeros((tokens, LANES), jnp.float32)
        weight = jnp.zeros((tokens, LANES), jnp.float32)
        for choice in range(TOP):
            same = info[:, choice : choice + 1] == target
            named = jnp.where(same, 1.0, named)
            weight = jnp.where(same, gates[:, TOP + choice : TOP + choice + 1], weight)
        rank = fdot(before, named.astype(jnp.bfloat16))
        chosen = jnp.where(rank == slot, named, 0.0)
        factors = chosen * weight
        high = factors.astype(jnp.bfloat16)
        factors_ref[source, :tokens] = high
        factors_ref[source, tokens:] = (factors - high.astype(jnp.float32)).astype(jnp.bfloat16)
        rows = fdot(chosen.astype(jnp.bfloat16), held[source, :, :half], ((0,), (0,)))
        rows = rows.astype(jnp.bfloat16)
        spot = pl.ds(pl.multiple_of(source * capacity, capacity), capacity)
        for number in range(side):
            outs[number][spot, :] = rows[number * capacity : (number + 1) * capacity, :]
        return carry

    lax.fori_loop(0, side, one_source, 0)


def project(chunks, weights, start, out_ref, begin):
    chunk, half = chunks[0].shape
    hidden = weights[0].shape[1]
    for first in range(0, len(chunks), 2):
        rows = jnp.concatenate([chunks[first][...], chunks[first + 1][...]], axis=0)
        for number, weight_ref in enumerate(weights):
            out_ref[
                begin + first * chunk : begin + (first + 2) * chunk,
                number * hidden : (number + 1) * hidden,
            ] = fdot(rows, weight_ref[pl.ds(start, half), :])


def early_kernel(lane_ref, *refs):
    number = (len(refs) - 4) // 2
    own, partner = refs[:number], refs[number : 2 * number]
    weights, own_out, partner_out = refs[2 * number : -2], refs[-2], refs[-1]
    half = own[0].shape[1]
    project(own, weights, pl.multiple_of(lane_ref[0] * half, half), own_out, 0)
    project(partner, weights, pl.multiple_of((1 - lane_ref[0]) * half, half), partner_out, 0)


def late_kernel(capacity, lane_ref, *refs):
    side = EXP_GRP
    number = side // 2
    own, partner = refs[:number], refs[number : 2 * number]
    weights, own_early, partner_early = refs[2 * number : -6], refs[-6], refs[-5]
    mine_ref, theirs_ref, own_late, partner_late = refs[-4:]
    chunk, half = own[0].shape
    hidden = mine_ref.shape[1]
    project(own, weights, pl.multiple_of(lane_ref[0] * half, half), own_late, 0)
    project(partner, weights, pl.multiple_of((1 - lane_ref[0]) * half, half), partner_late, 0)

    def block(index, first, second, owned, partnered):
        one, two = index // number, index % number
        left = pl.multiple_of(one * chunk + (second * number + two) * capacity, capacity)
        right = pl.multiple_of(two * chunk + (first * number + one) * capacity, capacity)
        both = owned[pl.ds(left, capacity), :] + partnered[pl.ds(right, capacity), :]
        gate, up = both[:, :hidden], both[:, hidden:]
        acts = (gate / (1.0 + jnp.exp(-gate)) * up).astype(jnp.bfloat16)
        far = number * chunk
        mine_ref[pl.ds(pl.multiple_of(first * far + left, capacity), capacity), :] = acts
        theirs_ref[pl.ds(pl.multiple_of(second * far + right, capacity), capacity), :] = acts

    def blocks(index, carry):
        for first, owned in ((0, own_early), (1, own_late)):
            for second, partnered in ((0, partner_early), (1, partner_late)):
                block(index, first, second, owned, partnered)
        return carry

    lax.fori_loop(0, number * number, blocks, 0)


def down_kernel(places, lane_ref, mine_ref, received_ref, down_ref, other_ref, *outs):
    chunk, half = outs[0].shape
    start = pl.multiple_of(lane_ref[0] * half, half)
    for place, out_ref in zip(places, outs):
        begin = place * chunk
        out_ref[...] = (
            fdot(mine_ref[begin : begin + chunk, :], down_ref[:, pl.ds(start, half)])
            + fdot(received_ref[begin : begin + chunk, :], other_ref[:, pl.ds(start, half)])
        ).astype(jnp.bfloat16)


def combine_kernel(capacity, *refs):
    side = EXP_GRP
    chunks, factors_ref, outs = refs[:side], refs[side], refs[side + 1 :]
    for source in range(side):
        rows = jnp.concatenate(
            [chunk[source * capacity : (source + 1) * capacity, :] for chunk in chunks], axis=0
        )
        both = fdot(factors_ref[source], rows)
        tokens = both.shape[0] // 2
        outs[source][...] = (both[:tokens] + both[tokens:]).astype(outs[source].dtype)


def layer(
    tokens_in, norm_gain, gate_proj, up_proj, down_proj, route_ids, group_weight, expert_weight
):
    token_count, model_width = tokens_in.shape
    expert_count = gate_proj.shape[0] * lax.axis_size("ep")
    lane_count = lax.axis_size("tp")
    part_width = model_width // lane_count
    hidden_width = gate_proj.shape[2]
    side = EXP_GRP
    capacity = min(token_count, max(2, 2 * token_count * TOP // expert_count))
    chunk = side * capacity
    order = (0, 4, 3, 5, 2, 6, 1, 7)
    lane_index = lax.axis_index("tp")
    lane = lane_index.reshape(1)
    place = lax.axis_index("ep")
    row, col = place // side, place % side
    deltas = jnp.asarray(order, jnp.int32)
    targets = jnp.where(
        lane_index == 0, row * side + (col + deltas) % side, ((row + deltas) % side) * side + col
    )
    swap = [(number, lane_count - 1 - number) for number in range(lane_count)]
    half_type = jnp.bfloat16

    other_down = lax.ppermute(down_proj[0], "tp", swap)
    (packed,) = call(
        prepare_kernel,
        [((token_count, part_width + LANES), half_type)],
        lane,
        tokens_in,
        norm_gain.reshape(1, model_width),
        route_ids.T,
        group_weight.T,
        expert_weight.T,
        scalars=1,
        far=True,
        scratch=[
            pltpu.VMEM((token_count, model_width), half_type),
            pltpu.VMEM((1, model_width), jnp.float32),
            pltpu.VMEM((TOP, token_count), jnp.int32),
            pltpu.VMEM((group_weight.shape[1], token_count), jnp.float32),
            pltpu.VMEM((TOP, token_count), jnp.float32),
            pltpu.SemaphoreType.DMA((5,)),
        ],
    )
    blocks = [packed]
    for delta in order[1:]:
        blocks.append(shift(packed, True, delta))
    *outgoing, factors = call(
        functools.partial(select_kernel, capacity),
        [((chunk, part_width), half_type)] * side
        + [((side, 2 * token_count, chunk), half_type)],
        targets,
        *blocks,
        scalars=1,
        scratch=[pltpu.VMEM((side,) + packed.shape, half_type)],
    )
    own = [outgoing[0]]
    for place, delta in enumerate(order[1:], 1):
        own.append(shift(outgoing[place], False, delta))
    partner = [lax.ppermute(rows, "tp", swap) for rows in own]
    number = side // 2
    weights = (gate_proj[0], up_proj[0])
    sums = ((number * chunk, 2 * hidden_width), jnp.float32)
    early = call(
        early_kernel, [sums] * 2, lane, *own[:number], *partner[:number], *weights, scalars=1
    )
    mine, theirs = call(
        functools.partial(late_kernel, capacity),
        [((side * chunk, hidden_width), half_type)] * 2,
        lane,
        *own[number:],
        *partner[number:],
        *weights,
        *early,
        scalars=1,
        scratch=[pltpu.VMEM(*sums)] * 2,
        limit=16,
    )
    received = lax.ppermute(theirs, "tp", swap)
    returned = [None] * side
    for some in ((1, 2, 3), (4, 5, 6, 7, 0)):
        results = call(
            functools.partial(down_kernel, some),
            [((chunk, part_width), half_type)] * len(some),
            lane,
            mine,
            received,
            down_proj[0],
            other_down,
            scalars=1,
        )
        for place, result in zip(some, results):
            returned[place] = shift(result, False, -order[place]) if place else result
    kept, *partials = call(
        functools.partial(combine_kernel, capacity),
        [((token_count, part_width), jnp.float32)]
        + [((token_count, part_width), half_type)] * (side - 1),
        *returned,
        factors,
    )
    total = kept
    for place, delta in enumerate(order[1:]):
        total += shift(partials[place], True, -delta).astype(jnp.float32)
    return total.astype(half_type)


def solution(mesh):
    in_specs = (
        P(("grp", "ep"), None),
        P(),
        P("ep", None, "tp"),
        P("ep", None, "tp"),
        P("ep", "tp", None),
        P(("grp", "ep"), None),
        P(("grp", "ep"), None),
        P(("grp", "ep"), None),
    )
    out_specs = P(("grp", "ep"), "tp")
    return jax.shard_map(layer, mesh=mesh, in_specs=in_specs, out_specs=out_specs, check_vma=False)
```

time: 216 us -> 146 us (0.68)
  blocking collectives: 80.2 us -> 0 us
  starting transfers between devices: 13.9 us -> 88.7 us
  waiting for transfers between devices: 80.4 us -> 34.1 us
  Pallas kernels: 0 us -> 14 us
  between operations: 13.6 us -> 0.18 us
  matrix products: 11.1 us -> 0 us
  other arithmetic: 9.82 us -> 1.48 us
    ppermute x0 -> x38, starting transfers between devices: none -> 88.7 us  [the longest x28 81.3 us: shift(): return lax.ppermute(array, AXES, shift_pairs(gathering, delta))]
    all_to_all x2 -> x0, blocking collectives: 80.2 us -> none  [the longest x1 72 us: on_device(): lax.all_to_all(outgoing.reshape(expert_count, capacity, part_width), 'ep'...]
    all_to_all x1 -> x0, waiting for transfers between devices: 51.9 us -> none  [on_device(): lax.all_to_all(results, 'ep', split_axis=0, concat_axis=0, tiled=True)]
    ppermute x0 -> x38, waiting for transfers between devices: none -> 34.1 us  [the longest x28 31.1 us: shift(): return lax.ppermute(array, AXES, shift_pairs(gathering, delta))]
    all_gather x1 -> x0, waiting for transfers between devices: 28.4 us -> none  [on_device(): column_piece = lax.all_gather(arrived, 'tp', axis=1, tiled=True)]
    pallas_call x0 -> x7, Pallas kernels: none -> 14 us  [call(): pl.pallas_call(kernel, out_shape=[jax.ShapeDtypeStruct(*output) for outpu...]
    all_to_all x1 -> x0, starting transfers between devices: 13.9 us -> none  [on_device(): lax.all_to_all(results, 'ep', split_axis=0, concat_axis=0, tiled=True)]
    dot_general x4 -> x0, matrix products: 11.1 us -> none  [the longest x1 5.32 us: on_device(): jnp.dot(column_piece, up_local, preferred_element_type=jnp.float32)]
  transfers between devices with their start and end apart: 2 -> 38, of which waited for: 2 -> 14; matrix products, arithmetic and copies ran while one was open for 0% -> 0% of each run, Pallas kernels for 0% -> 5%
where the time goes in v2:
time: 146 us; the launch traced here: 145 us
  starting transfers between devices  88.7 us (61%)
  waiting for transfers between devices  34.1 us (23%)
  Pallas kernels  14 us (10%)
  local copies, waits for them, and re-layouts  6.9 us (5%)
  other arithmetic  1.48 us (1%)
    ppermute x28, starting transfers between devices, shift(): return lax.ppermute(array, AXES, shift_pairs(gathering, delta))  81.3 us
    ppermute x28, waiting for transfers between devices, shift(): return lax.ppermute(array, AXES, shift_pairs(gathering, delta))  31.1 us
    pallas_call x7, Pallas kernels, call(): pl.pallas_call(kernel, out_shape=[jax.ShapeDtypeStruct(*output) for outpu...  14 us
    ppermute x8, starting transfers between devices, layer(): partner = [lax.ppermute(rows, 'tp', swap) for rows in own]  7.07 us
    unnamed x20, local copies, waits for them, and re-layouts  6.9 us
  transfers between devices with their start and end apart: 38, of which 14 were waited for; matrix products, arithmetic and copies ran while one was open for 0% of the time, Pallas kernels for 5%

profile of v2, /device:TPU:514, one launch (start us, length us, event | category | flops | bytes accessed | tf_op | source)
XLA Modules:
  0.0 145.4 jit_solution(3615492903842737533)
XLA Ops:
  4.0 12.0 %collective-permute-start.6 = (bf16[64,1152]{1,0:T(8,128)(2,1)S(1)}, bf16[64,1152]{1,0:T(8,128)(2,1)S(1)}, u32[]{:S(2)}, u32[]{:S(2)}) collective-permute-start(bf16[64,1152]{1,0:T(8,128)(2,1)S(1)} %shard_map.91.refs_0_), channel_id=1, source_target_pairs={{0,112},{1,15},{2,114},{3,1},{4,116},{5,3},{6,118},{7,5},{8,120},{... | collective-permute-start | bytes 442376 | tf_op jit(solution)/shard_map/ppermute | solution.py:35
  18.9 2.7 %collective-permute-start.2 = (bf16[64,1152]{1,0:T(8,128)(2,1)S(1)}, bf16[64,1152]{1,0:T(8,128)(2,1)S(1)}, u32[]{:S(2)}, u32[]{:S(2)}) collective-permute-start(bf16[64,1152]{1,0:T(8,128)(2,1)S(1)} %shard_map.91.refs_0_), channel_id=1, source_target_pairs={{0,80},{1,11},{2,82},{3,13},{4,84},{5,15},{6,86},{7,1},{8,88},{9,3... | collective-permute-start | bytes 442376 | tf_op jit(solution)/shard_map/ppermute | solution.py:35
  22.8 3.9 %collective-permute-start = (bf16[64,1152]{1,0:T(8,128)(2,1)S(1)}, bf16[64,1152]{1,0:T(8,128)(2,1)S(1)}, u32[]{:S(2)}, u32[]{:S(2)}) collective-permute-start(bf16[64,1152]{1,0:T(8,128)(2,1)S(1)} %shard_map.91.refs_0_), channel_id=1, source_target_pairs={{0,64},{1,9},{2,66},{3,11},{4,68},{5,13},{6,70},{7,15},{8,72},{9,1... | collective-permute-start | bytes 442376 | tf_op jit(solution)/shard_map/ppermute | solution.py:35
  27.3 7.3 %collective-permute-done.1.refs_2_ = bf16[64,1152]{1,0:T(8,128)(2,1)S(1)} collective-permute-done((bf16[64,1152]{1,0:T(8,128)(2,1)S(1)}, bf16[64,1152]{1,0:T(8,128)(2,1)S(1)}, u32[]{:S(2)}, u32[]{:S(2)}) %collective-permute-start.1) | collective-permute-done | bytes 147488 | tf_op jit(solution)/shard_map/ppermute | solution.py:35
  34.6 4.7 %shard_map.92 = (bf16[128,1024]{1,0:T(8,128)(2,1)S(1)}, bf16[128,1024]{1,0:T(8,128)(2,1)S(1)}, bf16[128,1024]{1,0:T(8,128)(2,1)S(1)}, bf16[128,1024]{1,0:T(8,128...) custom-call(s32[8]{0:T(128)S(1)} %broadcast_select_fusion.targets_re, ...), custom_call_target="tpu_custom_call" | custom-call | tf_op jit(solution)/shard_map/pallas_call | solution.py:42
  39.3 2.8 %collective-permute-start.7 = (bf16[128,1024]{1,0:T(8,128)(2,1)S(1)}, bf16[128,1024]{1,0:T(8,128)(2,1)S(1)}, u32[]{:S(2)}, u32[]{:S(2)}) collective-permute-start(bf16[128,1024]{1,0:T(8,128)(2,1)S(1)} %get-tuple-element.34), channel_id=1, source_target_pairs={{0,4},{1,33},{2,6},{3,35},{4,8},{5,37},{6,10},{7,39},{8,12},{9,41}... | collective-permute-start | bytes 786440 | tf_op jit(solution)/shard_map/ppermute | solution.py:35
  43.6 8.2 %collective-permute-start.9 = (bf16[128,1024]{1,0:T(8,128)(2,1)S(1)}, bf16[128,1024]{1,0:T(8,128)(2,1)S(1)}, u32[]{:S(2)}, u32[]{:S(2)}) collective-permute-start(bf16[128,1024]{1,0:T(8,128)(2,1)S(1)} %get-tuple-element.36), channel_id=1, source_target_pairs={{0,2},{1,17},{2,4},{3,19},{4,6},{5,21},{6,8},{7,23},{8,10},{9,25},... | collective-permute-start | bytes 786440 | tf_op jit(solution)/shard_map/ppermute | solution.py:35
  51.8 2.5 %collective-permute-start.10 = (bf16[128,1024]{1,0:T(8,128)(2,1)S(1)}, bf16[128,1024]{1,0:T(8,128)(2,1)S(1)}, u32[]{:S(2)}, u32[]{:S(2)}) collective-permute-start(bf16[128,1024]{1,0:T(8,128)(2,1)S(1)} %get-tuple-element.37), channel_id=1, source_target_pairs={{0,14},{1,113},{2,0},{3,115},{4,2},{5,117},{6,4},{7,119},{8,6},{9,... | collective-permute-start | bytes 786440 | tf_op jit(solution)/shard_map/ppermute | solution.py:35
  56.0 7.2 %collective-permute-start.16 = (bf16[128,1024]{1,0:T(8,128)(2,1)S(1)}, bf16[128,1024]{1,0:T(8,128)(2,1)S(1)}, u32[]{:S(2)}, u32[]{:S(2)}) collective-permute-start(bf16[128,1024]{1,0:T(8,128)(2,1)S(1)} %get-tuple-element.40), channel_id=1, source_target_pairs={{0,6},{1,49},{2,8},{3,51},{4,10},{5,53},{6,12},{7,55},{8,14},{9,57... | collective-permute-start | bytes 786440 | tf_op jit(solution)/shard_map/ppermute | solution.py:35
  64.7 5.6 %collective-permute-start.19 = (bf16[128,1024]{1,0:T(8,128)(2,1)S(1)}, bf16[128,1024]{1,0:T(8,128)(2,1)S(1)}, u32[]{:S(2)}, u32[]{:S(2)}) collective-permute-start(bf16[128,1024]{1,0:T(8,128)(2,1)S(1)} %collective-permute-done.15.refs_1_), channel_id=1, source_target_pairs={{0,1},{1,0},{2,3},{3,2},{4,5},{5,4},{6,7},{7,6},{8,9},{9,8},{10,11... | collective-permute-start | bytes 786440 | tf_op jit(solution)/shard_map/ppermute | solution.py:273
  71.8 3.6 %collective-permute-done.17.refs_3_ = bf16[128,1024]{1,0:T(8,128)(2,1)S(1)} collective-permute-done((bf16[128,1024]{1,0:T(8,128)(2,1)S(1)}, bf16[128,1024]{1,0:T(8,128)(2,1)S(1)}, u32[]{:S(2)}, u32[]{:S(2)}) %collective-permute-start.17) | collective-permute-done | bytes 262176 | tf_op jit(solution)/shard_map/ppermute | solution.py:35
  80.4 2.3 %shard_map.93 = (f32[512,1024]{1,0:T(8,128)S(1)}, f32[512,1024]{1,0:T(8,128)S(1)}) custom-call(s32[1]{0:T(128)} %bitcast.lane_ref, bf16[128,1024]{1,0:T(8,128)(2,1)S(1)} %get-tuple-element.38.refs_0_, bf16[128,1024]{1,0:T(8,128)(2,1)S(1)} %collective-permute-done.15.refs_1_, bf16[128,1024]{1,0:T(8,128)(2,1)S(1)} %collective-permute-done.16.refs_2_, ...), custom_call_target="tpu_custom_call" | custom-call | tf_op jit(solution)/shard_map/pallas_call | solution.py:42
  82.8 3.4 %shard_map.94 = (bf16[1024,512]{1,0:T(8,128)(2,1)S(1)}, bf16[1024,512]{1,0:T(8,128)(2,1)S(1)}) custom-call(s32[1]{0:T(128)} %bitcast.lane_ref, bf16[128,1024]{1,0:T(8,128)(2,1)S(1)} %collective-permute-done.7.refs_0_, bf16[128,1024]{1,0:T(8,128)(2,1)S(1)} %collective-permute-done.8.refs_1_, bf16[128,1024]{1,0:T(8,128)(2,1)S(1)} %collective-permute-done.9.refs_2_, ...), custom_call_target="tpu_custom_call" | custom-call | tf_op jit(solution)/shard_map/pallas_call | solution.py:42
  86.6 2.5 %collective-permute-done.22.received_ref = bf16[1024,512]{1,0:T(8,128)(2,1)S(1)} collective-permute-done((bf16[1024,512]{1,0:T(8,128)(2,1)S(1)}, bf16[1024,512]{1,0:T(8,128)(2,1)S(1)}, u32[]{:S(2)}, u32[]{:S(2)}) %collective-permute-start.22) | collective-permute-done | bytes 1048608 | tf_op jit(solution)/shard_map/ppermute | solution.py:292
  90.0 4.2 %collective-permute-start.24 = (bf16[128,1024]{1,0:T(8,128)(2,1)S(1)}, bf16[128,1024]{1,0:T(8,128)(2,1)S(1)}, u32[]{:S(2)}, u32[]{:S(2)}) collective-permute-start(bf16[128,1024]{1,0:T(8,128)(2,1)S(1)} %get-tuple-element.47), channel_id=1, source_target_pairs={{0,8},{1,65},{2,10},{3,67},{4,12},{5,69},{6,14},{7,71},{8,0},{9,73... | collective-permute-start | bytes 786440 | tf_op jit(solution)/shard_map/ppermute | solution.py:35
  95.5 3.8 %collective-permute-start.26 = (bf16[128,1024]{1,0:T(8,128)(2,1)S(1)}, bf16[128,1024]{1,0:T(8,128)(2,1)S(1)}, u32[]{:S(2)}, u32[]{:S(2)}) collective-permute-start(bf16[128,1024]{1,0:T(8,128)(2,1)S(1)} %get-tuple-element.49), channel_id=1, source_target_pairs={{0,6},{1,49},{2,8},{3,51},{4,10},{5,53},{6,12},{7,55},{8,14},{9,57... | collective-permute-start | bytes 786440 | tf_op jit(solution)/shard_map/ppermute | solution.py:35
  100.8 4.1 %collective-permute-start.27 = (bf16[128,1024]{1,0:T(8,128)(2,1)S(1)}, bf16[128,1024]{1,0:T(8,128)(2,1)S(1)}, u32[]{:S(2)}, u32[]{:S(2)}) collective-permute-start(bf16[128,1024]{1,0:T(8,128)(2,1)S(1)} %get-tuple-element.50), channel_id=1, source_target_pairs={{0,12},{1,97},{2,14},{3,99},{4,0},{5,101},{6,2},{7,103},{8,4},{9,1... | collective-permute-start | bytes 786440 | tf_op jit(solution)/shard_map/ppermute | solution.py:35
  107.3 3.9 %collective-permute-done.25.refs_2_ = bf16[128,1024]{1,0:T(8,128)(2,1)S(1)} collective-permute-done((bf16[128,1024]{1,0:T(8,128)(2,1)S(1)}, bf16[128,1024]{1,0:T(8,128)(2,1)S(1)}, u32[]{:S(2)}, u32[]{:S(2)}) %collective-permute-start.25) | collective-permute-done | bytes 262176 | tf_op jit(solution)/shard_map/ppermute | solution.py:35
  112.8 2.7 %collective-permute-done.27.refs_4_ = bf16[128,1024]{1,0:T(8,128)(2,1)S(1)} collective-permute-done((bf16[128,1024]{1,0:T(8,128)(2,1)S(1)}, bf16[128,1024]{1,0:T(8,128)(2,1)S(1)}, u32[]{:S(2)}, u32[]{:S(2)}) %collective-permute-start.27) | collective-permute-done | bytes 262176 | tf_op jit(solution)/shard_map/ppermute | solution.py:35
  115.5 3.6 %collective-permute-done.28.refs_5_ = bf16[128,1024]{1,0:T(8,128)(2,1)S(1)} collective-permute-done((bf16[128,1024]{1,0:T(8,128)(2,1)S(1)}, bf16[128,1024]{1,0:T(8,128)(2,1)S(1)}, u32[]{:S(2)}, u32[]{:S(2)}) %collective-permute-start.28) | collective-permute-done | bytes 262176 | tf_op jit(solution)/shard_map/ppermute | solution.py:35
  121.8 6.4 %collective-permute-start.31 = (bf16[64,1024]{1,0:T(8,128)(2,1)S(1)}, bf16[64,1024]{1,0:T(8,128)(2,1)S(1)}, u32[]{:S(2)}, u32[]{:S(2)}) collective-permute-start(bf16[64,1024]{1,0:T(8,128)(2,1)S(1)} %get-tuple-element.56), channel_id=1, source_target_pairs={{0,64},{1,9},{2,66},{3,11},{4,68},{5,13},{6,70},{7,15},{8,72},{9,1... | collective-permute-start | bytes 393224 | tf_op jit(solution)/shard_map/ppermute | solution.py:35
  128.2 3.8 %collective-permute-start.33 = (bf16[64,1024]{1,0:T(8,128)(2,1)S(1)}, bf16[64,1024]{1,0:T(8,128)(2,1)S(1)}, u32[]{:S(2)}, u32[]{:S(2)}) collective-permute-start(bf16[64,1024]{1,0:T(8,128)(2,1)S(1)} %get-tuple-element.58), channel_id=1, source_target_pairs={{0,48},{1,7},{2,50},{3,9},{4,52},{5,11},{6,54},{7,13},{8,56},{9,15... | collective-permute-start | bytes 393224 | tf_op jit(solution)/shard_map/ppermute | solution.py:35
  132.0 3.6 %collective-permute-start.34 = (bf16[64,1024]{1,0:T(8,128)(2,1)S(1)}, bf16[64,1024]{1,0:T(8,128)(2,1)S(1)}, u32[]{:S(2)}, u32[]{:S(2)}) collective-permute-start(bf16[64,1024]{1,0:T(8,128)(2,1)S(1)} %get-tuple-element.59), channel_id=1, source_target_pairs={{0,96},{1,13},{2,98},{3,15},{4,100},{5,1},{6,102},{7,3},{8,104},{9... | collective-permute-start | bytes 393224 | tf_op jit(solution)/shard_map/ppermute | solution.py:35
  139.6 4.5 %collective-permute-done.35 = bf16[64,1024]{1,0:T(8,128)(2,1)S(1)} collective-permute-done((bf16[64,1024]{1,0:T(8,128)(2,1)S(1)}, bf16[64,1024]{1,0:T(8,128)(2,1)S(1)}, u32[]{:S(2)}, u32[]{:S(2)}) %collective-permute-start.35) | collective-permute-done | bytes 131104 | tf_op jit(solution)/shard_map/ppermute | solution.py:35
  (81 shorter events, 36.0 us)
Async XLA Ops:
  4.0 17.6 %collective-permute-start.6 = (bf16[64,1152]{1,0:T(8,128)(2,1)S(1)}, bf16[64,1152]{1,0:T(8,128)(2,1)S(1)}, u32[]{:S(2)}, u32[]{:S(2)}) collective-permute-start(bf16[64,1152]{1,0:T(8,128)(2,1)S(1)} %shard_map.91.refs_0_), channel_id=1, source_target_pairs={{0,112},{1,15},{2,114},{3,1},{4,116},{5,3},{6,118},{7,5},{8,120},{... | collective-permute-start | bytes 442376 | tf_op jit(solution)/shard_map/ppermute | solution.py:35
  16.0 11.3 %collective-permute-start.4 = (bf16[64,1152]{1,0:T(8,128)(2,1)S(1)}, bf16[64,1152]{1,0:T(8,128)(2,1)S(1)}, u32[]{:S(2)}, u32[]{:S(2)}) collective-permute-start(bf16[64,1152]{1,0:T(8,128)(2,1)S(1)} %shard_map.91.refs_0_), channel_id=1, source_target_pairs={{0,96},{1,13},{2,98},{3,15},{4,100},{5,1},{6,102},{7,3},{8,104},{9... | collective-permute-start | bytes 442376 | tf_op jit(solution)/shard_map/ppermute | solution.py:35
  17.6 9.7 %collective-permute-start.3 = (bf16[64,1152]{1,0:T(8,128)(2,1)S(1)}, bf16[64,1152]{1,0:T(8,128)(2,1)S(1)}, u32[]{:S(2)}, u32[]{:S(2)}) collective-permute-start(bf16[64,1152]{1,0:T(8,128)(2,1)S(1)} %shard_map.91.refs_0_), channel_id=1, source_target_pairs={{0,32},{1,5},{2,34},{3,7},{4,36},{5,9},{6,38},{7,11},{8,40},{9,13}... | collective-permute-start | bytes 442376 | tf_op jit(solution)/shard_map/ppermute | solution.py:35
  21.6 13.0 %collective-permute-start.1 = (bf16[64,1152]{1,0:T(8,128)(2,1)S(1)}, bf16[64,1152]{1,0:T(8,128)(2,1)S(1)}, u32[]{:S(2)}, u32[]{:S(2)}) collective-permute-start(bf16[64,1152]{1,0:T(8,128)(2,1)S(1)} %shard_map.91.refs_0_), channel_id=1, source_target_pairs={{0,48},{1,7},{2,50},{3,9},{4,52},{5,11},{6,54},{7,13},{8,56},{9,15... | collective-permute-start | bytes 442376 | tf_op jit(solution)/shard_map/ppermute | solution.py:35
  22.8 11.8 %collective-permute-start = (bf16[64,1152]{1,0:T(8,128)(2,1)S(1)}, bf16[64,1152]{1,0:T(8,128)(2,1)S(1)}, u32[]{:S(2)}, u32[]{:S(2)}) collective-permute-start(bf16[64,1152]{1,0:T(8,128)(2,1)S(1)} %shard_map.91.refs_0_), channel_id=1, source_target_pairs={{0,64},{1,9},{2,66},{3,11},{4,68},{5,13},{6,70},{7,15},{8,72},{9,1... | collective-permute-start | bytes 442376 | tf_op jit(solution)/shard_map/ppermute | solution.py:35
  39.3 15.0 %collective-permute-start.7 = (bf16[128,1024]{1,0:T(8,128)(2,1)S(1)}, bf16[128,1024]{1,0:T(8,128)(2,1)S(1)}, u32[]{:S(2)}, u32[]{:S(2)}) collective-permute-start(bf16[128,1024]{1,0:T(8,128)(2,1)S(1)} %get-tuple-element.34), channel_id=1, source_target_pairs={{0,4},{1,33},{2,6},{3,35},{4,8},{5,37},{6,10},{7,39},{8,12},{9,41}... | collective-permute-start | bytes 786440 | tf_op jit(solution)/shard_map/ppermute | solution.py:35
  42.1 13.8 %collective-permute-start.8 = (bf16[128,1024]{1,0:T(8,128)(2,1)S(1)}, bf16[128,1024]{1,0:T(8,128)(2,1)S(1)}, u32[]{:S(2)}, u32[]{:S(2)}) collective-permute-start(bf16[128,1024]{1,0:T(8,128)(2,1)S(1)} %get-tuple-element.35), channel_id=1, source_target_pairs={{0,12},{1,97},{2,14},{3,99},{4,0},{5,101},{6,2},{7,103},{8,4},{9,1... | collective-permute-start | bytes 786440 | tf_op jit(solution)/shard_map/ppermute | solution.py:35
  43.6 19.6 %collective-permute-start.9 = (bf16[128,1024]{1,0:T(8,128)(2,1)S(1)}, bf16[128,1024]{1,0:T(8,128)(2,1)S(1)}, u32[]{:S(2)}, u32[]{:S(2)}) collective-permute-start(bf16[128,1024]{1,0:T(8,128)(2,1)S(1)} %get-tuple-element.36), channel_id=1, source_target_pairs={{0,2},{1,17},{2,4},{3,19},{4,6},{5,21},{6,8},{7,23},{8,10},{9,25},... | collective-permute-start | bytes 786440 | tf_op jit(solution)/shard_map/ppermute | solution.py:35
  51.8 37.3 %collective-permute-start.23 = (bf16[512,2048]{1,0:T(8,128)(2,1)}, bf16[512,2048]{1,0:T(8,128)(2,1)S(1)}, u32[]{:S(2)}, u32[]{:S(2)}) collective-permute-start(bf16[512,2048]{1,0:T(8,128)(2,1)} %bitcast.8), channel_id=1, source_target_pairs={{0,1},{1,0},{2,3},{3,2},{4,5},{5,4},{6,7},{7,6},{8,9},{9,8},{10,11... | collective-permute-start | bytes 6291464 | tf_op jit(solution)/shard_map/ppermute | solution.py:237
  51.8 11.4 %collective-permute-start.10 = (bf16[128,1024]{1,0:T(8,128)(2,1)S(1)}, bf16[128,1024]{1,0:T(8,128)(2,1)S(1)}, u32[]{:S(2)}, u32[]{:S(2)}) collective-permute-start(bf16[128,1024]{1,0:T(8,128)(2,1)S(1)} %get-tuple-element.37), channel_id=1, source_target_pairs={{0,14},{1,113},{2,0},{3,115},{4,2},{5,117},{6,4},{7,119},{8,6},{9,... | collective-permute-start | bytes 786440 | tf_op jit(solution)/shard_map/ppermute | solution.py:35
  54.3 10.4 %collective-permute-start.15 = (bf16[128,1024]{1,0:T(8,128)(2,1)S(1)}, bf16[128,1024]{1,0:T(8,128)(2,1)S(1)}, u32[]{:S(2)}, u32[]{:S(2)}) collective-permute-start(bf16[128,1024]{1,0:T(8,128)(2,1)S(1)} %get-tuple-element.39), channel_id=1, source_target_pairs={{0,8},{1,65},{2,10},{3,67},{4,12},{5,69},{6,14},{7,71},{8,0},{9,73... | collective-permute-start | bytes 786440 | tf_op jit(solution)/shard_map/ppermute | solution.py:35
  56.0 15.8 %collective-permute-start.16 = (bf16[128,1024]{1,0:T(8,128)(2,1)S(1)}, bf16[128,1024]{1,0:T(8,128)(2,1)S(1)}, u32[]{:S(2)}, u32[]{:S(2)}) collective-permute-start(bf16[128,1024]{1,0:T(8,128)(2,1)S(1)} %get-tuple-element.40), channel_id=1, source_target_pairs={{0,6},{1,49},{2,8},{3,51},{4,10},{5,53},{6,12},{7,55},{8,14},{9,57... | collective-permute-start | bytes 786440 | tf_op jit(solution)/shard_map/ppermute | solution.py:35
  63.1 12.2 %collective-permute-start.17 = (bf16[128,1024]{1,0:T(8,128)(2,1)S(1)}, bf16[128,1024]{1,0:T(8,128)(2,1)S(1)}, u32[]{:S(2)}, u32[]{:S(2)}) collective-permute-start(bf16[128,1024]{1,0:T(8,128)(2,1)S(1)} %get-tuple-element.41), channel_id=1, source_target_pairs={{0,10},{1,81},{2,12},{3,83},{4,14},{5,85},{6,0},{7,87},{8,2},{9,89... | collective-permute-start | bytes 786440 | tf_op jit(solution)/shard_map/ppermute | solution.py:35
  63.2 12.5 %collective-permute-start.18 = (bf16[128,1024]{1,0:T(8,128)(2,1)S(1)}, bf16[128,1024]{1,0:T(8,128)(2,1)S(1)}, u32[]{:S(2)}, u32[]{:S(2)}) collective-permute-start(bf16[128,1024]{1,0:T(8,128)(2,1)S(1)} %get-tuple-element.38.refs_0_), channel_id=1, source_target_pairs={{0,1},{1,0},{2,3},{3,2},{4,5},{5,4},{6,7},{7,6},{8,9},{9,8},{10,11... | collective-permute-start | bytes 786440 | tf_op jit(solution)/shard_map/ppermute | solution.py:273
  64.7 11.2 %collective-permute-start.19 = (bf16[128,1024]{1,0:T(8,128)(2,1)S(1)}, bf16[128,1024]{1,0:T(8,128)(2,1)S(1)}, u32[]{:S(2)}, u32[]{:S(2)}) collective-permute-start(bf16[128,1024]{1,0:T(8,128)(2,1)S(1)} %collective-permute-done.15.refs_1_), channel_id=1, source_target_pairs={{0,1},{1,0},{2,3},{3,2},{4,5},{5,4},{6,7},{7,6},{8,9},{9,8},{10,11... | collective-permute-start | bytes 786440 | tf_op jit(solution)/shard_map/ppermute | solution.py:273
  90.0 14.9 %collective-permute-start.24 = (bf16[128,1024]{1,0:T(8,128)(2,1)S(1)}, bf16[128,1024]{1,0:T(8,128)(2,1)S(1)}, u32[]{:S(2)}, u32[]{:S(2)}) collective-permute-start(bf16[128,1024]{1,0:T(8,128)(2,1)S(1)} %get-tuple-element.47), channel_id=1, source_target_pairs={{0,8},{1,65},{2,10},{3,67},{4,12},{5,69},{6,14},{7,71},{8,0},{9,73... | collective-permute-start | bytes 786440 | tf_op jit(solution)/shard_map/ppermute | solution.py:35
  94.3 16.9 %collective-permute-start.25 = (bf16[128,1024]{1,0:T(8,128)(2,1)S(1)}, bf16[128,1024]{1,0:T(8,128)(2,1)S(1)}, u32[]{:S(2)}, u32[]{:S(2)}) collective-permute-start(bf16[128,1024]{1,0:T(8,128)(2,1)S(1)} %get-tuple-element.48), channel_id=1, source_target_pairs={{0,10},{1,81},{2,12},{3,83},{4,14},{5,85},{6,0},{7,87},{8,2},{9,89... | collective-permute-start | bytes 786440 | tf_op jit(solution)/shard_map/ppermute | solution.py:35
  95.5 17.3 %collective-permute-start.26 = (bf16[128,1024]{1,0:T(8,128)(2,1)S(1)}, bf16[128,1024]{1,0:T(8,128)(2,1)S(1)}, u32[]{:S(2)}, u32[]{:S(2)}) collective-permute-start(bf16[128,1024]{1,0:T(8,128)(2,1)S(1)} %get-tuple-element.49), channel_id=1, source_target_pairs={{0,6},{1,49},{2,8},{3,51},{4,10},{5,53},{6,12},{7,55},{8,14},{9,57... | collective-permute-start | bytes 786440 | tf_op jit(solution)/shard_map/ppermute | solution.py:35
  100.8 14.7 %collective-permute-start.27 = (bf16[128,1024]{1,0:T(8,128)(2,1)S(1)}, bf16[128,1024]{1,0:T(8,128)(2,1)S(1)}, u32[]{:S(2)}, u32[]{:S(2)}) collective-permute-start(bf16[128,1024]{1,0:T(8,128)(2,1)S(1)} %get-tuple-element.50), channel_id=1, source_target_pairs={{0,12},{1,97},{2,14},{3,99},{4,0},{5,101},{6,2},{7,103},{8,4},{9,1... | collective-permute-start | bytes 786440 | tf_op jit(solution)/shard_map/ppermute | solution.py:35
  104.9 14.1 %collective-permute-start.28 = (bf16[128,1024]{1,0:T(8,128)(2,1)S(1)}, bf16[128,1024]{1,0:T(8,128)(2,1)S(1)}, u32[]{:S(2)}, u32[]{:S(2)}) collective-permute-start(bf16[128,1024]{1,0:T(8,128)(2,1)S(1)} %get-tuple-element.51), channel_id=1, source_target_pairs={{0,4},{1,33},{2,6},{3,35},{4,8},{5,37},{6,10},{7,39},{8,12},{9,41}... | collective-permute-start | bytes 786440 | tf_op jit(solution)/shard_map/ppermute | solution.py:35
  104.9 15.2 %collective-permute-start.29 = (bf16[128,1024]{1,0:T(8,128)(2,1)S(1)}, bf16[128,1024]{1,0:T(8,128)(2,1)S(1)}, u32[]{:S(2)}, u32[]{:S(2)}) collective-permute-start(bf16[128,1024]{1,0:T(8,128)(2,1)S(1)} %get-tuple-element.52), channel_id=1, source_target_pairs={{0,14},{1,113},{2,0},{3,115},{4,2},{5,117},{6,4},{7,119},{8,6},{9,... | collective-permute-start | bytes 786440 | tf_op jit(solution)/shard_map/ppermute | solution.py:35
  111.1 9.9 %collective-permute-start.30 = (bf16[128,1024]{1,0:T(8,128)(2,1)S(1)}, bf16[128,1024]{1,0:T(8,128)(2,1)S(1)}, u32[]{:S(2)}, u32[]{:S(2)}) collective-permute-start(bf16[128,1024]{1,0:T(8,128)(2,1)S(1)} %get-tuple-element.53), channel_id=1, source_target_pairs={{0,2},{1,17},{2,4},{3,19},{4,6},{5,21},{6,8},{7,23},{8,10},{9,25},... | collective-permute-start | bytes 786440 | tf_op jit(solution)/shard_map/ppermute | solution.py:35
  121.8 13.8 %collective-permute-start.31 = (bf16[64,1024]{1,0:T(8,128)(2,1)S(1)}, bf16[64,1024]{1,0:T(8,128)(2,1)S(1)}, u32[]{:S(2)}, u32[]{:S(2)}) collective-permute-start(bf16[64,1024]{1,0:T(8,128)(2,1)S(1)} %get-tuple-element.56), channel_id=1, source_target_pairs={{0,64},{1,9},{2,66},{3,11},{4,68},{5,13},{6,70},{7,15},{8,72},{9,1... | collective-permute-start | bytes 393224 | tf_op jit(solution)/shard_map/ppermute | solution.py:35
  128.2 11.2 %collective-permute-start.33 = (bf16[64,1024]{1,0:T(8,128)(2,1)S(1)}, bf16[64,1024]{1,0:T(8,128)(2,1)S(1)}, u32[]{:S(2)}, u32[]{:S(2)}) collective-permute-start(bf16[64,1024]{1,0:T(8,128)(2,1)S(1)} %get-tuple-element.58), channel_id=1, source_target_pairs={{0,48},{1,7},{2,50},{3,9},{4,52},{5,11},{6,54},{7,13},{8,56},{9,15... | collective-permute-start | bytes 393224 | tf_op jit(solution)/shard_map/ppermute | solution.py:35
  (24 other events, 109.2 us)

commit v3 on v2

v3 whole, which is shorter than its diff:
```python
import functools

import jax
import jax.numpy as jnp
from jax import lax
from jax.experimental import pallas as pl
from jax.experimental.pallas import tpu as pltpu
from jax.sharding import PartitionSpec as P


TOP = 8
EXP_GRP = 8
LANES = 128

EPSILON = 1e-06
AXES = ("ep", "tp")
ORDER = (0, 4, 3, 5, 2, 6, 1, 7)
EARLY = 4


def shift_pairs(gathering, delta):
    lanes = lax.axis_size("tp")
    side = EXP_GRP
    pairs = []
    for device in range(lax.axis_size("ep")):
        row, col = divmod(device, side)
        for lane in range(lanes):
            if (lane == 0) == gathering:
                target = ((row + delta) % side) * side + col
            else:
                target = row * side + (col + delta) % side
            pairs.append((device * lanes + lane, target * lanes + lane))
    return pairs


def shift(array, gathering, delta):
    return lax.ppermute(array, AXES, shift_pairs(gathering, delta))


def call(kernel, outputs, *operands, scalars=0, scratch=(), far=0, limit=8):
    smem = pl.BlockSpec(memory_space=pltpu.SMEM)
    vmem = pl.BlockSpec(memory_space=pltpu.VMEM)
    hbm = pl.BlockSpec(memory_space=pltpu.HBM)
    near = len(operands) - far
    operands = operands[:near] + tuple(
        pltpu.with_memory_space_constraint(operand, pltpu.HBM) for operand in operands[near:]
    )
    return pl.pallas_call(
        kernel,
        out_shape=[jax.ShapeDtypeStruct(*output) for output in outputs],
        in_specs=[smem] * scalars + [vmem] * (near - scalars) + [hbm] * far,
        out_specs=[vmem] * len(outputs),
        scratch_shapes=list(scratch),
        compiler_params=pltpu.CompilerParams(vmem_limit_bytes=limit << 20),
    )(*operands)


def fdot(left, right, contract=((1,), (0,))):
    return lax.dot_general(left, right, (contract, ((), ())), preferred_element_type=jnp.float32)


def prepare_kernel(lane_ref, *refs):
    far, out_ref, near, sems = refs[:5], refs[5], refs[6:11], refs[11]
    copies = [pltpu.make_async_copy(far[n], near[n], sems.at[n]) for n in range(5)]
    for copy in copies:
        copy.start()
    for copy in copies:
        copy.wait()
    tokens_ref, gain_ref, ids_ref, group_ref, expert_ref = near
    half = out_ref.shape[1]
    count, width = tokens_ref.shape
    values = tokens_ref[...].astype(jnp.float32)
    mean = jnp.sum(values * values, axis=1, keepdims=True) / width
    scale = lax.rsqrt(mean + EPSILON)
    start = pl.multiple_of(lane_ref[0] * half, half)
    own = tokens_ref[:, pl.ds(start, half)].astype(jnp.float32)
    out_ref[:count, :] = (own * scale * gain_ref[:, pl.ds(start, half)]).astype(jnp.bfloat16)
    ids = ids_ref[...]
    group_ids = lax.div(ids, jnp.full_like(ids, EXP_GRP))
    part = jnp.zeros(ids.shape, jnp.float32)
    for group in range(group_ref.shape[0]):
        part += jnp.where(group_ids == group, group_ref[group : group + 1, :], 0.0)
    weights = expert_ref[...]
    gates = part * weights / jnp.sum(weights, axis=0, keepdims=True)
    high = gates.astype(jnp.bfloat16)
    rest = gates - high.astype(jnp.float32)
    middle = rest.astype(jnp.bfloat16)
    lowest = (rest - middle.astype(jnp.float32)).astype(jnp.bfloat16)
    out_ref[count:, :] = jnp.zeros((TOP, half), jnp.bfloat16)
    for number, term in enumerate((ids.astype(jnp.float32).astype(jnp.bfloat16), high, middle, lowest)):
        out_ref[count:, number * LANES : number * LANES + count] = term


def chosen_slots(order, lane_ref, place_ref, blocks):
    side = EXP_GRP
    tokens = blocks[0].shape[0] - TOP
    lane, place = lane_ref[0], place_ref[0]
    row, col = lax.div(place, side), lax.rem(place, side)
    line = lax.broadcasted_iota(jnp.int32, (side, tokens), 0)
    target = jnp.zeros((side, tokens), jnp.int32)
    for number, delta in enumerate(order):
        along = row * side + lax.rem(col + delta, side)
        across = lax.rem(row + delta, side) * side + col
        target = jnp.where(line == number, (1 - lane) * along + lane * across, target)
    target = target.astype(jnp.float32)
    named, gates = [], []
    for source in range(side):
        info = blocks[source][tokens:, : 4 * LANES].astype(jnp.float32)
        ids = info[:, :tokens]
        terms = [info[:, n * LANES : n * LANES + tokens] for n in range(1, 4)]
        weights = terms[0] + terms[1] + terms[2]
        match = jnp.zeros((side, tokens), jnp.float32)
        gate = jnp.zeros((side, tokens), jnp.float32)
        for choice in range(TOP):
            same = ids[choice : choice + 1, :] == target
            match = jnp.where(same, 1.0, match)
            gate = jnp.where(same, weights[choice : choice + 1, :], gate)
        named.append(match)
        gates.append(gate)
    named = jnp.concatenate(named, axis=0)
    first = lax.broadcasted_iota(jnp.int32, (tokens, tokens), 0)
    second = lax.broadcasted_iota(jnp.int32, (tokens, tokens), 1)
    before = (first < second).astype(jnp.float32).astype(jnp.bfloat16)
    rank = fdot(named.astype(jnp.bfloat16), before)
    return jnp.where(named > 0.0, rank, -1.0), gates


def select_kernel(capacity, order, lane_ref, place_ref, *refs):
    side = EXP_GRP
    blocks, outs = refs[:side], refs[side:]
    tokens = blocks[0].shape[0] - TOP
    slots, _ = chosen_slots(order, lane_ref, place_ref, blocks)
    slot = lax.broadcasted_iota(jnp.int32, (capacity, tokens), 0).astype(jnp.float32)
    for source in range(side):
        lines = [slots[source * side + n : source * side + n + 1, :] for n in range(side)]
        chosen = jnp.concatenate([(line == slot).astype(jnp.float32) for line in lines], axis=0)
        rows = fdot(chosen.astype(jnp.bfloat16), blocks[source][:tokens, :]).astype(jnp.bfloat16)
        for number in range(side):
            outs[number][source * capacity : (source + 1) * capacity, :] = rows[
                number * capacity : (number + 1) * capacity, :
            ]


def factors_kernel(capacity, order, lane_ref, place_ref, *refs):
    side = EXP_GRP
    blocks, weights = refs[:side], refs[side : side + 2]
    out_ref, held, sems = refs[side + 2], refs[side + 3 : side + 5], refs[side + 5]
    copies = [pltpu.make_async_copy(weights[n], held[n], sems.at[n]) for n in range(2)]
    for copy in copies:
        copy.start()
    tokens = blocks[0].shape[0] - TOP
    slots, gates = chosen_slots(order, lane_ref, place_ref, blocks)
    slot = lax.broadcasted_iota(jnp.int32, (capacity, tokens), 0).astype(jnp.float32)
    for source in range(side):
        factors = jnp.concatenate(
            [
                jnp.where(
                    slots[source * side + n : source * side + n + 1, :] == slot,
                    gates[source][n : n + 1, :],
                    0.0,
                )
                for n in range(side)
            ],
            axis=0,
        ).T
        high = factors.astype(jnp.bfloat16)
        out_ref[source, :tokens] = high
        out_ref[source, tokens:] = (factors - high.astype(jnp.float32)).astype(jnp.bfloat16)
    for copy in copies:
        copy.wait()


def project(chunks, weights, start, out_ref, begin):
    chunk, half = chunks[0].shape
    hidden = weights[0].shape[1]
    for first in range(0, len(chunks), 2):
        pair = chunks[first : first + 2]
        rows = jnp.concatenate([part[...] for part in pair], axis=0)
        for number, weight_ref in enumerate(weights):
            out_ref[
                begin + first * chunk : begin + (first + len(pair)) * chunk,
                number * hidden : (number + 1) * hidden,
            ] = fdot(rows, weight_ref[pl.ds(start, half), :])


def early_kernel(lane_ref, *refs):
    own, partner = refs[:EARLY], refs[EARLY : 2 * EARLY]
    weights, own_out, partner_out = refs[2 * EARLY : -2], refs[-2], refs[-1]
    half = own[0].shape[1]
    project(own, weights, pl.multiple_of(lane_ref[0] * half, half), own_out, 0)
    project(partner, weights, pl.multiple_of((1 - lane_ref[0]) * half, half), partner_out, 0)


def late_kernel(capacity, lane_ref, *refs):
    side = EXP_GRP
    late = side - EARLY
    own, partner = refs[:late], refs[late : 2 * late]
    weights, own_early, partner_early = refs[2 * late : -7], refs[-7], refs[-6]
    mine_ref, own_late, partner_late = refs[-5], refs[-2], refs[-1]
    theirs_refs = refs[-4:-2]
    chunk, half = own[0].shape
    hidden = mine_ref.shape[1]
    project(own, weights, pl.multiple_of(lane_ref[0] * half, half), own_late, 0)
    project(partner, weights, pl.multiple_of((1 - lane_ref[0]) * half, half), partner_late, 0)
    rows = ((0, EARLY, own_early), (EARLY, late, own_late))
    cols = ((0, EARLY, partner_early, theirs_refs[0]), (EARLY, late, partner_late, theirs_refs[1]))
    for base, count, owned in rows:
        for far_base, far_count, partnered, theirs_ref in cols:

            def block(index, carry):
                one = lax.div(index, far_count)
                two = index - one * far_count
                left = pl.multiple_of(one * chunk + (far_base + two) * capacity, capacity)
                right = pl.multiple_of(two * chunk + (base + one) * capacity, capacity)
                both = owned[pl.ds(left, capacity), :] + partnered[pl.ds(right, capacity), :]
                gate, up = both[:, :hidden], both[:, hidden:]
                acts = (gate / (1.0 + jnp.exp(-gate)) * up).astype(jnp.bfloat16)
                whole = pl.multiple_of(base * chunk + left, capacity)
                mine_ref[pl.ds(whole, capacity), :] = acts
                theirs_ref[pl.ds(right, capacity), :] = acts
                return carry

            lax.fori_loop(0, count * far_count, block, 0, unroll=2)


def down_kernel(places, lane_ref, mine_ref, near_ref, far_ref, down_ref, other_ref, *outs):
    chunk, half = outs[0].shape
    start = pl.multiple_of(lane_ref[0] * half, half)
    for place, out_ref in zip(places, outs):
        begin = place * chunk
        received_ref = far_ref if place >= EARLY else near_ref
        at = begin - EARLY * chunk if place >= EARLY else begin
        out_ref[...] = (
            fdot(mine_ref[begin : begin + chunk, :], down_ref[:, pl.ds(start, half)])
            + fdot(received_ref[at : at + chunk, :], other_ref[:, pl.ds(start, half)])
        ).astype(jnp.bfloat16)


def combine_kernel(capacity, *refs):
    side = EXP_GRP
    chunks, factors_ref, outs = refs[:side], refs[side], refs[side + 1 :]
    for source in range(side):
        rows = jnp.concatenate(
            [chunk[source * capacity : (source + 1) * capacity, :] for chunk in chunks], axis=0
        )
        both = fdot(factors_ref[source], rows)
        tokens = both.shape[0] // 2
        outs[source][...] = (both[:tokens] + both[tokens:]).astype(outs[source].dtype)


def layer(
    tokens_in, norm_gain, gate_proj, up_proj, down_proj, route_ids, group_weight, expert_weight
):
    token_count, model_width = tokens_in.shape
    expert_count = gate_proj.shape[0] * lax.axis_size("ep")
    lane_count = lax.axis_size("tp")
    part_width = model_width // lane_count
    hidden_width = gate_proj.shape[2]
    side = EXP_GRP
    capacity = min(token_count, max(2, 2 * token_count * TOP // expert_count))
    chunk = side * capacity
    order = ORDER
    lane_index = lax.axis_index("tp")
    lane = lane_index.reshape(1)
    place = lax.axis_index("ep")
    spot = place.reshape(1)
    swap = [(number, lane_count - 1 - number) for number in range(lane_count)]
    half_type = jnp.bfloat16

    other_down = lax.ppermute(down_proj[0], "tp", swap)
    (packed,) = call(
        prepare_kernel,
        [((token_count + TOP, part_width), half_type)],
        lane,
        tokens_in,
        norm_gain.reshape(1, model_width),
        route_ids.T,
        group_weight.T,
        expert_weight.T,
        scalars=1,
        far=5,
        scratch=[
            pltpu.VMEM((token_count, model_width), half_type),
            pltpu.VMEM((1, model_width), jnp.float32),
            pltpu.VMEM((TOP, token_count), jnp.int32),
            pltpu.VMEM((group_weight.shape[1], token_count), jnp.float32),
            pltpu.VMEM((TOP, token_count), jnp.float32),
            pltpu.SemaphoreType.DMA((5,)),
        ],
    )
    blocks = [packed]
    for delta in order[1:]:
        blocks.append(shift(packed, True, delta))
    outgoing = call(
        functools.partial(select_kernel, capacity, order),
        [((chunk, part_width), half_type)] * side,
        lane,
        spot,
        *blocks,
        scalars=2,
    )
    factors, *weights = call(
        functools.partial(factors_kernel, capacity, order),
        [((side, 2 * token_count, chunk), half_type)]
        + [((model_width, hidden_width), half_type)] * 2,
        lane,
        spot,
        *blocks,
        gate_proj[0],
        up_proj[0],
        scalars=2,
        scratch=[pltpu.SemaphoreType.DMA((2,))],
        far=2,
    )
    own = [outgoing[0]]
    for place, delta in enumerate(order[1:], 1):
        own.append(shift(outgoing[place], False, delta))
    partner = []
    for delta, rows in zip(order, own):
        partner.append(lax.ppermute(rows, "tp", swap))
    sums = ((EARLY * chunk, 2 * hidden_width), jnp.float32)
    early = call(
        early_kernel, [sums] * 2, lane, *own[:EARLY], *partner[:EARLY], *weights, scalars=1
    )
    late = side - EARLY
    mine, *theirs = call(
        functools.partial(late_kernel, capacity),
        [
            ((side * chunk, hidden_width), half_type),
            ((EARLY * chunk, hidden_width), half_type),
            ((late * chunk, hidden_width), half_type),
        ],
        lane,
        *own[EARLY:],
        *partner[EARLY:],
        *weights,
        *early,
        scalars=1,
        scratch=[pltpu.VMEM((late * chunk, 2 * hidden_width), jnp.float32)] * 2,
        limit=16,
    )
    near = lax.ppermute(theirs[0], "tp", swap)
    far = lax.ppermute(theirs[1], "tp", swap)
    returned = [None] * side
    for some in (tuple(range(1, EARLY)), tuple(range(EARLY, side)) + (0,)):
        results = call(
            functools.partial(down_kernel, some),
            [((chunk, part_width), half_type)] * len(some),
            lane,
            mine,
            near,
            far if some[0] >= EARLY else near,
            down_proj[0],
            other_down,
            scalars=1,
        )
        for place, result in zip(some, results):
            returned[place] = shift(result, False, -order[place]) if place else result
    kept, *partials = call(
        functools.partial(combine_kernel, capacity),
        [((token_count, part_width), jnp.float32)]
        + [((token_count, part_width), half_type)] * (side - 1),
        *returned,
        factors,
    )
    total = kept
    for place, delta in enumerate(order[1:]):
        total += shift(partials[place], True, -delta).astype(jnp.float32)
    return total.astype(half_type)


def solution(mesh):
    in_specs = (
        P(("grp", "ep"), None),
        P(),
        P("ep", None, "tp"),
        P("ep", None, "tp"),
        P("ep", "tp", None),
        P(("grp", "ep"), None),
        P(("grp", "ep"), None),
        P(("grp", "ep"), None),
    )
    out_specs = P(("grp", "ep"), "tp")
    return jax.shard_map(layer, mesh=mesh, in_specs=in_specs, out_specs=out_specs, check_vma=False)
```

time: 146 us -> 137 us (0.938)
  local copies, waits for them, and re-layouts: 6.9 us -> 0.01 us
    unnamed x20 -> x2, local copies, waits for them, and re-layouts: 6.9 us -> 0.01 us
    ppermute x9 -> x10, starting transfers between devices: 7.39 us -> 2.17 us  [the longest x8 1.54 us: layer(): partner.append(lax.ppermute(rows, 'tp', swap))]
    ppermute x28, starting transfers between devices: 81.3 us -> 85.5 us  [shift(): return lax.ppermute(array, AXES, shift_pairs(gathering, delta))]
    ppermute x28, waiting for transfers between devices: 31.1 us -> 33.2 us  [shift(): return lax.ppermute(array, AXES, shift_pairs(gathering, delta))]
    ppermute x9 -> x10, waiting for transfers between devices: 2.98 us -> 1.42 us  [the longest x1 1.4 us: layer(): near = lax.ppermute(theirs[0], 'tp', swap)]
    pallas_call x7 -> x8, Pallas kernels: 14 us -> 13.7 us  [call(): pl.pallas_call(kernel, out_shape=[jax.ShapeDtypeStruct(*output) for outpu...]
  transfers between devices with their start and end apart: 38 -> 39, of which waited for: 14 -> 16; matrix products, arithmetic and copies ran while one was open for 0% -> 0% of each run, Pallas kernels for 5% -> 9%
where the time goes in v3:
time: 137 us
  starting transfers between devices  87.7 us (64%)
  waiting for transfers between devices  34.6 us (25%)
  Pallas kernels  13.7 us (10%)
    ppermute x28, starting transfers between devices, shift(): return lax.ppermute(array, AXES, shift_pairs(gathering, delta))  85.5 us
    ppermute x28, waiting for transfers between devices, shift(): return lax.ppermute(array, AXES, shift_pairs(gathering, delta))  33.2 us
    pallas_call x8, Pallas kernels, call(): pl.pallas_call(kernel, out_shape=[jax.ShapeDtypeStruct(*output) for outpu...  13.7 us
  transfers between devices with their start and end apart: 39, of which 16 were waited for; matrix products, arithmetic and copies ran while one was open for 0% of the time, Pallas kernels for 9%

profile of v3, /device:TPU:514, one launch (start us, length us, event | category | flops | bytes accessed | tf_op | source)
XLA Modules:
  0.0 136.9 jit_solution(1064626558385427665)
XLA Ops:
  1.2 10.7 %collective-permute-start = (bf16[72,1024]{1,0:T(8,128)(2,1)S(1)}, bf16[72,1024]{1,0:T(8,128)(2,1)S(1)}, u32[]{:S(2)}, u32[]{:S(2)}) collective-permute-start(bf16[72,1024]{1,0:T(8,128)(2,1)S(1)} %shard_map.82.refs_0_), channel_id=1, source_target_pairs={{0,64},{1,9},{2,66},{3,11},{4,68},{5,13},{6,70},{7,15},{8,72},{9,1... | collective-permute-start | bytes 442376 | tf_op jit(solution)/shard_map/ppermute | solution.py:37
  11.9 4.5 %collective-permute-start.1 = (bf16[72,1024]{1,0:T(8,128)(2,1)S(1)}, bf16[72,1024]{1,0:T(8,128)(2,1)S(1)}, u32[]{:S(2)}, u32[]{:S(2)}) collective-permute-start(bf16[72,1024]{1,0:T(8,128)(2,1)S(1)} %shard_map.82.refs_0_), channel_id=1, source_target_pairs={{0,48},{1,7},{2,50},{3,9},{4,52},{5,11},{6,54},{7,13},{8,56},{9,15... | collective-permute-start | bytes 442376 | tf_op jit(solution)/shard_map/ppermute | solution.py:37
  16.9 3.2 %collective-permute-start.3 = (bf16[72,1024]{1,0:T(8,128)(2,1)S(1)}, bf16[72,1024]{1,0:T(8,128)(2,1)S(1)}, u32[]{:S(2)}, u32[]{:S(2)}) collective-permute-start(bf16[72,1024]{1,0:T(8,128)(2,1)S(1)} %shard_map.82.refs_0_), channel_id=1, source_target_pairs={{0,32},{1,5},{2,34},{3,7},{4,36},{5,9},{6,38},{7,11},{8,40},{9,13}... | collective-permute-start | bytes 442376 | tf_op jit(solution)/shard_map/ppermute | solution.py:37
  24.1 3.7 %collective-permute-start.6 = (bf16[72,1024]{1,0:T(8,128)(2,1)S(1)}, bf16[72,1024]{1,0:T(8,128)(2,1)S(1)}, u32[]{:S(2)}, u32[]{:S(2)}) collective-permute-start(bf16[72,1024]{1,0:T(8,128)(2,1)S(1)} %shard_map.82.refs_0_), channel_id=1, source_target_pairs={{0,112},{1,15},{2,114},{3,1},{4,116},{5,3},{6,118},{7,5},{8,120},{... | collective-permute-start | bytes 442376 | tf_op jit(solution)/shard_map/ppermute | solution.py:37
  29.3 2.2 %collective-permute-done.6.refs_7_ = bf16[72,1024]{1,0:T(8,128)(2,1)S(1)} collective-permute-done((bf16[72,1024]{1,0:T(8,128)(2,1)S(1)}, bf16[72,1024]{1,0:T(8,128)(2,1)S(1)}, u32[]{:S(2)}, u32[]{:S(2)}) %collective-permute-start.6) | collective-permute-done | bytes 147488 | tf_op jit(solution)/shard_map/ppermute | solution.py:37
  32.4 5.2 %collective-permute-start.15 = (bf16[128,1024]{1,0:T(8,128)(2,1)S(1)}, bf16[128,1024]{1,0:T(8,128)(2,1)S(1)}, u32[]{:S(2)}, u32[]{:S(2)}) collective-permute-start(bf16[128,1024]{1,0:T(8,128)(2,1)S(1)} %get-tuple-element.44), channel_id=1, source_target_pairs={{0,8},{1,65},{2,10},{3,67},{4,12},{5,69},{6,14},{7,71},{8,0},{9,73... | collective-permute-start | bytes 786440 | tf_op jit(solution)/shard_map/ppermute | solution.py:37
  37.7 9.6 %collective-permute-start.16 = (bf16[128,1024]{1,0:T(8,128)(2,1)S(1)}, bf16[128,1024]{1,0:T(8,128)(2,1)S(1)}, u32[]{:S(2)}, u32[]{:S(2)}) collective-permute-start(bf16[128,1024]{1,0:T(8,128)(2,1)S(1)} %get-tuple-element.45), channel_id=1, source_target_pairs={{0,6},{1,49},{2,8},{3,51},{4,10},{5,53},{6,12},{7,55},{8,14},{9,57... | collective-permute-start | bytes 786440 | tf_op jit(solution)/shard_map/ppermute | solution.py:37
  48.2 8.4 %collective-permute-done.16.refs_2_ = bf16[128,1024]{1,0:T(8,128)(2,1)S(1)} collective-permute-done((bf16[128,1024]{1,0:T(8,128)(2,1)S(1)}, bf16[128,1024]{1,0:T(8,128)(2,1)S(1)}, u32[]{:S(2)}, u32[]{:S(2)}) %collective-permute-start.16) | collective-permute-done | bytes 262176 | tf_op jit(solution)/shard_map/ppermute | solution.py:37
  56.6 4.9 %collective-permute-start.8 = (bf16[128,1024]{1,0:T(8,128)(2,1)S(1)}, bf16[128,1024]{1,0:T(8,128)(2,1)S(1)}, u32[]{:S(2)}, u32[]{:S(2)}) collective-permute-start(bf16[128,1024]{1,0:T(8,128)(2,1)S(1)} %get-tuple-element.38), channel_id=1, source_target_pairs={{0,12},{1,97},{2,14},{3,99},{4,0},{5,101},{6,2},{7,103},{8,4},{9,1... | collective-permute-start | bytes 786440 | tf_op jit(solution)/shard_map/ppermute | solution.py:37
  63.5 4.6 %collective-permute-done.8.refs_1_ = bf16[128,1024]{1,0:T(8,128)(2,1)S(1)} collective-permute-done((bf16[128,1024]{1,0:T(8,128)(2,1)S(1)}, bf16[128,1024]{1,0:T(8,128)(2,1)S(1)}, u32[]{:S(2)}, u32[]{:S(2)}) %collective-permute-start.8) | collective-permute-done | bytes 262176 | tf_op jit(solution)/shard_map/ppermute | solution.py:37
  68.6 2.3 %collective-permute-done.10.refs_3_ = bf16[128,1024]{1,0:T(8,128)(2,1)S(1)} collective-permute-done((bf16[128,1024]{1,0:T(8,128)(2,1)S(1)}, bf16[128,1024]{1,0:T(8,128)(2,1)S(1)}, u32[]{:S(2)}, u32[]{:S(2)}) %collective-permute-start.10) | collective-permute-done | bytes 262176 | tf_op jit(solution)/shard_map/ppermute | solution.py:37
  72.0 2.3 %shard_map.84 = (bf16[8,128,128]{2,1,0:T(8,128)(2,1)S(1)}, bf16[2048,512]{1,0:T(8,128)(2,1)S(1)}, bf16[2048,512]{1,0:T(8,128)(2,1)S(1)}) custom-call(s32[1]{0:T(128)} %bitcast.lane_ref, s32[1]{0:T(128)} %bitcast.1.place_ref, bf16[72,1024]{1,0:T(8,128)(2,1)S(1)} %shard_map.82.refs_0_, bf16[72,1024]{1,0:T(8,128)(2,1)S(1)} %collective-permute-done.refs_1_, ...), custom_call_target="tpu_custom_call" | custom-call | tf_op jit(solution)/shard_map/pallas_call | solution.py:48
  74.3 2.4 %shard_map.85 = (f32[512,1024]{1,0:T(8,128)S(1)}, f32[512,1024]{1,0:T(8,128)S(1)}) custom-call(s32[1]{0:T(128)} %bitcast.lane_ref, bf16[128,1024]{1,0:T(8,128)(2,1)S(1)} %get-tuple-element.43.refs_0_, bf16[128,1024]{1,0:T(8,128)(2,1)S(1)} %collective-permute-done.15.refs_1_, bf16[128,1024]{1,0:T(8,128)(2,1)S(1)} %collective-permute-done.16.refs_2_, ...), custom_call_target="tpu_custom_call" | custom-call | tf_op jit(solution)/shard_map/pallas_call | solution.py:48
  76.7 3.7 %shard_map.86 = (bf16[1024,512]{1,0:T(8,128)(2,1)S(1)}, bf16[512,512]{1,0:T(8,128)(2,1)S(1)}, bf16[512,512]{1,0:T(8,128)(2,1)S(1)}) custom-call(s32[1]{0:T(128)} %bitcast.lane_ref, bf16[128,1024]{1,0:T(8,128)(2,1)S(1)} %collective-permute-done.7.refs_0_, bf16[128,1024]{1,0:T(8,128)(2,1)S(1)} %collective-permute-done.8.refs_1_, ...), custom_call_target="tpu_custom_call" | custom-call | tf_op jit(solution)/shard_map/pallas_call | solution.py:48
  83.4 5.4 %collective-permute-start.25 = (bf16[128,1024]{1,0:T(8,128)(2,1)S(1)}, bf16[128,1024]{1,0:T(8,128)(2,1)S(1)}, u32[]{:S(2)}, u32[]{:S(2)}) collective-permute-start(bf16[128,1024]{1,0:T(8,128)(2,1)S(1)} %get-tuple-element.53), channel_id=1, source_target_pairs={{0,8},{1,65},{2,10},{3,67},{4,12},{5,69},{6,14},{7,71},{8,0},{9,73... | collective-permute-start | bytes 786440 | tf_op jit(solution)/shard_map/ppermute | solution.py:37
  88.8 5.0 %collective-permute-start.27 = (bf16[128,1024]{1,0:T(8,128)(2,1)S(1)}, bf16[128,1024]{1,0:T(8,128)(2,1)S(1)}, u32[]{:S(2)}, u32[]{:S(2)}) collective-permute-start(bf16[128,1024]{1,0:T(8,128)(2,1)S(1)} %get-tuple-element.55), channel_id=1, source_target_pairs={{0,6},{1,49},{2,8},{3,51},{4,10},{5,53},{6,12},{7,55},{8,14},{9,57... | collective-permute-start | bytes 786440 | tf_op jit(solution)/shard_map/ppermute | solution.py:37
  95.6 2.9 %collective-permute-start.29 = (bf16[128,1024]{1,0:T(8,128)(2,1)S(1)}, bf16[128,1024]{1,0:T(8,128)(2,1)S(1)}, u32[]{:S(2)}, u32[]{:S(2)}) collective-permute-start(bf16[128,1024]{1,0:T(8,128)(2,1)S(1)} %get-tuple-element.57), channel_id=1, source_target_pairs={{0,4},{1,33},{2,6},{3,35},{4,8},{5,37},{6,10},{7,39},{8,12},{9,41}... | collective-permute-start | bytes 786440 | tf_op jit(solution)/shard_map/ppermute | solution.py:37
  100.3 6.2 %collective-permute-start.31 = (bf16[128,1024]{1,0:T(8,128)(2,1)S(1)}, bf16[128,1024]{1,0:T(8,128)(2,1)S(1)}, u32[]{:S(2)}, u32[]{:S(2)}) collective-permute-start(bf16[128,1024]{1,0:T(8,128)(2,1)S(1)} %get-tuple-element.59), channel_id=1, source_target_pairs={{0,2},{1,17},{2,4},{3,19},{4,6},{5,21},{6,8},{7,23},{8,10},{9,25},... | collective-permute-start | bytes 786440 | tf_op jit(solution)/shard_map/ppermute | solution.py:37
  108.1 2.8 %collective-permute-done.29.refs_5_ = bf16[128,1024]{1,0:T(8,128)(2,1)S(1)} collective-permute-done((bf16[128,1024]{1,0:T(8,128)(2,1)S(1)}, bf16[128,1024]{1,0:T(8,128)(2,1)S(1)}, u32[]{:S(2)}, u32[]{:S(2)}) %collective-permute-start.29) | collective-permute-done | bytes 262176 | tf_op jit(solution)/shard_map/ppermute | solution.py:37
  113.6 3.5 %collective-permute-start.32 = (bf16[64,1024]{1,0:T(8,128)(2,1)S(1)}, bf16[64,1024]{1,0:T(8,128)(2,1)S(1)}, u32[]{:S(2)}, u32[]{:S(2)}) collective-permute-start(bf16[64,1024]{1,0:T(8,128)(2,1)S(1)} %get-tuple-element.62), channel_id=1, source_target_pairs={{0,64},{1,9},{2,66},{3,11},{4,68},{5,13},{6,70},{7,15},{8,72},{9,1... | collective-permute-start | bytes 393224 | tf_op jit(solution)/shard_map/ppermute | solution.py:37
  117.1 4.1 %collective-permute-start.33 = (bf16[64,1024]{1,0:T(8,128)(2,1)S(1)}, bf16[64,1024]{1,0:T(8,128)(2,1)S(1)}, u32[]{:S(2)}, u32[]{:S(2)}) collective-permute-start(bf16[64,1024]{1,0:T(8,128)(2,1)S(1)} %get-tuple-element.63), channel_id=1, source_target_pairs={{0,80},{1,11},{2,82},{3,13},{4,84},{5,15},{6,86},{7,1},{8,88},{9,3... | collective-permute-start | bytes 393224 | tf_op jit(solution)/shard_map/ppermute | solution.py:37
  121.2 4.3 %collective-permute-start.35 = (bf16[64,1024]{1,0:T(8,128)(2,1)S(1)}, bf16[64,1024]{1,0:T(8,128)(2,1)S(1)}, u32[]{:S(2)}, u32[]{:S(2)}) collective-permute-start(bf16[64,1024]{1,0:T(8,128)(2,1)S(1)} %get-tuple-element.65), channel_id=1, source_target_pairs={{0,96},{1,13},{2,98},{3,15},{4,100},{5,1},{6,102},{7,3},{8,104},{9... | collective-permute-start | bytes 393224 | tf_op jit(solution)/shard_map/ppermute | solution.py:37
  125.6 4.4 %collective-permute-start.37 = (bf16[64,1024]{1,0:T(8,128)(2,1)S(1)}, bf16[64,1024]{1,0:T(8,128)(2,1)S(1)}, u32[]{:S(2)}, u32[]{:S(2)}) collective-permute-start(bf16[64,1024]{1,0:T(8,128)(2,1)S(1)} %get-tuple-element.67), channel_id=1, source_target_pairs={{0,112},{1,15},{2,114},{3,1},{4,116},{5,3},{6,118},{7,5},{8,120},{... | collective-permute-start | bytes 393224 | tf_op jit(solution)/shard_map/ppermute | solution.py:37
  132.2 2.3 %collective-permute-done.36 = bf16[64,1024]{1,0:T(8,128)(2,1)S(1)} collective-permute-done((bf16[64,1024]{1,0:T(8,128)(2,1)S(1)}, bf16[64,1024]{1,0:T(8,128)(2,1)S(1)}, u32[]{:S(2)}, u32[]{:S(2)}) %collective-permute-start.36) | collective-permute-done | bytes 131104 | tf_op jit(solution)/shard_map/ppermute | solution.py:37
  (65 shorter events, 28.1 us)
Async XLA Ops:
  0.0 82.4 %collective-permute-start.24 = (bf16[512,2048]{1,0:T(8,128)(2,1)}, bf16[512,2048]{1,0:T(8,128)(2,1)S(1)}, u32[]{:S(2)}, u32[]{:S(2)}) collective-permute-start(bf16[512,2048]{1,0:T(8,128)(2,1)} %bitcast.9), channel_id=1, source_target_pairs={{0,1},{1,0},{2,3},{3,2},{4,5},{5,4},{6,7},{7,6},{8,9},{9,8},{10,11... | collective-permute-start | bytes 6291464 | tf_op jit(solution)/shard_map/ppermute | solution.py:270
  1.2 19.0 %collective-permute-start = (bf16[72,1024]{1,0:T(8,128)(2,1)S(1)}, bf16[72,1024]{1,0:T(8,128)(2,1)S(1)}, u32[]{:S(2)}, u32[]{:S(2)}) collective-permute-start(bf16[72,1024]{1,0:T(8,128)(2,1)S(1)} %shard_map.82.refs_0_), channel_id=1, source_target_pairs={{0,64},{1,9},{2,66},{3,11},{4,68},{5,13},{6,70},{7,15},{8,72},{9,1... | collective-permute-start | bytes 442376 | tf_op jit(solution)/shard_map/ppermute | solution.py:37
  11.9 11.1 %collective-permute-start.1 = (bf16[72,1024]{1,0:T(8,128)(2,1)S(1)}, bf16[72,1024]{1,0:T(8,128)(2,1)S(1)}, u32[]{:S(2)}, u32[]{:S(2)}) collective-permute-start(bf16[72,1024]{1,0:T(8,128)(2,1)S(1)} %shard_map.82.refs_0_), channel_id=1, source_target_pairs={{0,48},{1,7},{2,50},{3,9},{4,52},{5,11},{6,54},{7,13},{8,56},{9,15... | collective-permute-start | bytes 442376 | tf_op jit(solution)/shard_map/ppermute | solution.py:37
  16.9 10.8 %collective-permute-start.3 = (bf16[72,1024]{1,0:T(8,128)(2,1)S(1)}, bf16[72,1024]{1,0:T(8,128)(2,1)S(1)}, u32[]{:S(2)}, u32[]{:S(2)}) collective-permute-start(bf16[72,1024]{1,0:T(8,128)(2,1)S(1)} %shard_map.82.refs_0_), channel_id=1, source_target_pairs={{0,32},{1,5},{2,34},{3,7},{4,36},{5,9},{6,38},{7,11},{8,40},{9,13}... | collective-permute-start | bytes 442376 | tf_op jit(solution)/shard_map/ppermute | solution.py:37
  32.4 14.9 %collective-permute-start.15 = (bf16[128,1024]{1,0:T(8,128)(2,1)S(1)}, bf16[128,1024]{1,0:T(8,128)(2,1)S(1)}, u32[]{:S(2)}, u32[]{:S(2)}) collective-permute-start(bf16[128,1024]{1,0:T(8,128)(2,1)S(1)} %get-tuple-element.44), channel_id=1, source_target_pairs={{0,8},{1,65},{2,10},{3,67},{4,12},{5,69},{6,14},{7,71},{8,0},{9,73... | collective-permute-start | bytes 786440 | tf_op jit(solution)/shard_map/ppermute | solution.py:37
  37.7 18.9 %collective-permute-start.16 = (bf16[128,1024]{1,0:T(8,128)(2,1)S(1)}, bf16[128,1024]{1,0:T(8,128)(2,1)S(1)}, u32[]{:S(2)}, u32[]{:S(2)}) collective-permute-start(bf16[128,1024]{1,0:T(8,128)(2,1)S(1)} %get-tuple-element.45), channel_id=1, source_target_pairs={{0,6},{1,49},{2,8},{3,51},{4,10},{5,53},{6,12},{7,55},{8,14},{9,57... | collective-permute-start | bytes 786440 | tf_op jit(solution)/shard_map/ppermute | solution.py:37
  47.3 14.1 %collective-permute-start.17 = (bf16[128,1024]{1,0:T(8,128)(2,1)S(1)}, bf16[128,1024]{1,0:T(8,128)(2,1)S(1)}, u32[]{:S(2)}, u32[]{:S(2)}) collective-permute-start(bf16[128,1024]{1,0:T(8,128)(2,1)S(1)} %get-tuple-element.46), channel_id=1, source_target_pairs={{0,10},{1,81},{2,12},{3,83},{4,14},{5,85},{6,0},{7,87},{8,2},{9,89... | collective-permute-start | bytes 786440 | tf_op jit(solution)/shard_map/ppermute | solution.py:37
  47.3 14.1 %collective-permute-start.18 = (bf16[128,1024]{1,0:T(8,128)(2,1)S(1)}, bf16[128,1024]{1,0:T(8,128)(2,1)S(1)}, u32[]{:S(2)}, u32[]{:S(2)}) collective-permute-start(bf16[128,1024]{1,0:T(8,128)(2,1)S(1)} %get-tuple-element.43.refs_0_), channel_id=1, source_target_pairs={{0,1},{1,0},{2,3},{3,2},{4,5},{5,4},{6,7},{7,6},{8,9},{9,8},{10,11... | collective-permute-start | bytes 786440 | tf_op jit(solution)/shard_map/ppermute | solution.py:320
  47.3 16.2 %collective-permute-start.7 = (bf16[128,1024]{1,0:T(8,128)(2,1)S(1)}, bf16[128,1024]{1,0:T(8,128)(2,1)S(1)}, u32[]{:S(2)}, u32[]{:S(2)}) collective-permute-start(bf16[128,1024]{1,0:T(8,128)(2,1)S(1)} %get-tuple-element.37), channel_id=1, source_target_pairs={{0,4},{1,33},{2,6},{3,35},{4,8},{5,37},{6,10},{7,39},{8,12},{9,41}... | collective-permute-start | bytes 786440 | tf_op jit(solution)/shard_map/ppermute | solution.py:37
  56.6 11.5 %collective-permute-start.8 = (bf16[128,1024]{1,0:T(8,128)(2,1)S(1)}, bf16[128,1024]{1,0:T(8,128)(2,1)S(1)}, u32[]{:S(2)}, u32[]{:S(2)}) collective-permute-start(bf16[128,1024]{1,0:T(8,128)(2,1)S(1)} %get-tuple-element.38), channel_id=1, source_target_pairs={{0,12},{1,97},{2,14},{3,99},{4,0},{5,101},{6,2},{7,103},{8,4},{9,1... | collective-permute-start | bytes 786440 | tf_op jit(solution)/shard_map/ppermute | solution.py:37
  61.5 9.5 %collective-permute-start.10 = (bf16[128,1024]{1,0:T(8,128)(2,1)S(1)}, bf16[128,1024]{1,0:T(8,128)(2,1)S(1)}, u32[]{:S(2)}, u32[]{:S(2)}) collective-permute-start(bf16[128,1024]{1,0:T(8,128)(2,1)S(1)} %get-tuple-element.40), channel_id=1, source_target_pairs={{0,14},{1,113},{2,0},{3,115},{4,2},{5,117},{6,4},{7,119},{8,6},{9,... | collective-permute-start | bytes 786440 | tf_op jit(solution)/shard_map/ppermute | solution.py:37
  80.6 13.3 %collective-permute-start.23 = (bf16[512,512]{1,0:T(8,128)(2,1)S(1)}, bf16[512,512]{1,0:T(8,128)(2,1)S(1)}, u32[]{:S(2)}, u32[]{:S(2)}) collective-permute-start(bf16[512,512]{1,0:T(8,128)(2,1)S(1)} %get-tuple-element.51), channel_id=1, source_target_pairs={{0,1},{1,0},{2,3},{3,2},{4,5},{5,4},{6,7},{7,6},{8,9},{9,8},{10,11... | collective-permute-start | bytes 1572872 | tf_op jit(solution)/shard_map/ppermute | solution.py:343
  83.4 16.8 %collective-permute-start.25 = (bf16[128,1024]{1,0:T(8,128)(2,1)S(1)}, bf16[128,1024]{1,0:T(8,128)(2,1)S(1)}, u32[]{:S(2)}, u32[]{:S(2)}) collective-permute-start(bf16[128,1024]{1,0:T(8,128)(2,1)S(1)} %get-tuple-element.53), channel_id=1, source_target_pairs={{0,8},{1,65},{2,10},{3,67},{4,12},{5,69},{6,14},{7,71},{8,0},{9,73... | collective-permute-start | bytes 786440 | tf_op jit(solution)/shard_map/ppermute | solution.py:37
  88.8 11.4 %collective-permute-start.26 = (bf16[128,1024]{1,0:T(8,128)(2,1)S(1)}, bf16[128,1024]{1,0:T(8,128)(2,1)S(1)}, u32[]{:S(2)}, u32[]{:S(2)}) collective-permute-start(bf16[128,1024]{1,0:T(8,128)(2,1)S(1)} %get-tuple-element.54), channel_id=1, source_target_pairs={{0,10},{1,81},{2,12},{3,83},{4,14},{5,85},{6,0},{7,87},{8,2},{9,89... | collective-permute-start | bytes 786440 | tf_op jit(solution)/shard_map/ppermute | solution.py:37
  88.8 17.6 %collective-permute-start.27 = (bf16[128,1024]{1,0:T(8,128)(2,1)S(1)}, bf16[128,1024]{1,0:T(8,128)(2,1)S(1)}, u32[]{:S(2)}, u32[]{:S(2)}) collective-permute-start(bf16[128,1024]{1,0:T(8,128)(2,1)S(1)} %get-tuple-element.55), channel_id=1, source_target_pairs={{0,6},{1,49},{2,8},{3,51},{4,10},{5,53},{6,12},{7,55},{8,14},{9,57... | collective-permute-start | bytes 786440 | tf_op jit(solution)/shard_map/ppermute | solution.py:37
  95.5 12.6 %collective-permute-start.28 = (bf16[128,1024]{1,0:T(8,128)(2,1)S(1)}, bf16[128,1024]{1,0:T(8,128)(2,1)S(1)}, u32[]{:S(2)}, u32[]{:S(2)}) collective-permute-start(bf16[128,1024]{1,0:T(8,128)(2,1)S(1)} %get-tuple-element.56), channel_id=1, source_target_pairs={{0,12},{1,97},{2,14},{3,99},{4,0},{5,101},{6,2},{7,103},{8,4},{9,1... | collective-permute-start | bytes 786440 | tf_op jit(solution)/shard_map/ppermute | solution.py:37
  95.6 15.3 %collective-permute-start.29 = (bf16[128,1024]{1,0:T(8,128)(2,1)S(1)}, bf16[128,1024]{1,0:T(8,128)(2,1)S(1)}, u32[]{:S(2)}, u32[]{:S(2)}) collective-permute-start(bf16[128,1024]{1,0:T(8,128)(2,1)S(1)} %get-tuple-element.57), channel_id=1, source_target_pairs={{0,4},{1,33},{2,6},{3,35},{4,8},{5,37},{6,10},{7,39},{8,12},{9,41}... | collective-permute-start | bytes 786440 | tf_op jit(solution)/shard_map/ppermute | solution.py:37
  100.3 12.6 %collective-permute-start.30 = (bf16[128,1024]{1,0:T(8,128)(2,1)S(1)}, bf16[128,1024]{1,0:T(8,128)(2,1)S(1)}, u32[]{:S(2)}, u32[]{:S(2)}) collective-permute-start(bf16[128,1024]{1,0:T(8,128)(2,1)S(1)} %get-tuple-element.58), channel_id=1, source_target_pairs={{0,14},{1,113},{2,0},{3,115},{4,2},{5,117},{6,4},{7,119},{8,6},{9,... | collective-permute-start | bytes 786440 | tf_op jit(solution)/shard_map/ppermute | solution.py:37
  100.3 12.6 %collective-permute-start.31 = (bf16[128,1024]{1,0:T(8,128)(2,1)S(1)}, bf16[128,1024]{1,0:T(8,128)(2,1)S(1)}, u32[]{:S(2)}, u32[]{:S(2)}) collective-permute-start(bf16[128,1024]{1,0:T(8,128)(2,1)S(1)} %get-tuple-element.59), channel_id=1, source_target_pairs={{0,2},{1,17},{2,4},{3,19},{4,6},{5,21},{6,8},{7,23},{8,10},{9,25},... | collective-permute-start | bytes 786440 | tf_op jit(solution)/shard_map/ppermute | solution.py:37
  113.6 12.0 %collective-permute-start.32 = (bf16[64,1024]{1,0:T(8,128)(2,1)S(1)}, bf16[64,1024]{1,0:T(8,128)(2,1)S(1)}, u32[]{:S(2)}, u32[]{:S(2)}) collective-permute-start(bf16[64,1024]{1,0:T(8,128)(2,1)S(1)} %get-tuple-element.62), channel_id=1, source_target_pairs={{0,64},{1,9},{2,66},{3,11},{4,68},{5,13},{6,70},{7,15},{8,72},{9,1... | collective-permute-start | bytes 393224 | tf_op jit(solution)/shard_map/ppermute | solution.py:37
  117.1 12.8 %collective-permute-start.33 = (bf16[64,1024]{1,0:T(8,128)(2,1)S(1)}, bf16[64,1024]{1,0:T(8,128)(2,1)S(1)}, u32[]{:S(2)}, u32[]{:S(2)}) collective-permute-start(bf16[64,1024]{1,0:T(8,128)(2,1)S(1)} %get-tuple-element.63), channel_id=1, source_target_pairs={{0,80},{1,11},{2,82},{3,13},{4,84},{5,15},{6,86},{7,1},{8,88},{9,3... | collective-permute-start | bytes 393224 | tf_op jit(solution)/shard_map/ppermute | solution.py:37
  121.2 10.9 %collective-permute-start.34 = (bf16[64,1024]{1,0:T(8,128)(2,1)S(1)}, bf16[64,1024]{1,0:T(8,128)(2,1)S(1)}, u32[]{:S(2)}, u32[]{:S(2)}) collective-permute-start(bf16[64,1024]{1,0:T(8,128)(2,1)S(1)} %get-tuple-element.64), channel_id=1, source_target_pairs={{0,48},{1,7},{2,50},{3,9},{4,52},{5,11},{6,54},{7,13},{8,56},{9,15... | collective-permute-start | bytes 393224 | tf_op jit(solution)/shard_map/ppermute | solution.py:37
  121.2 10.9 %collective-permute-start.35 = (bf16[64,1024]{1,0:T(8,128)(2,1)S(1)}, bf16[64,1024]{1,0:T(8,128)(2,1)S(1)}, u32[]{:S(2)}, u32[]{:S(2)}) collective-permute-start(bf16[64,1024]{1,0:T(8,128)(2,1)S(1)} %get-tuple-element.65), channel_id=1, source_target_pairs={{0,96},{1,13},{2,98},{3,15},{4,100},{5,1},{6,102},{7,3},{8,104},{9... | collective-permute-start | bytes 393224 | tf_op jit(solution)/shard_map/ppermute | solution.py:37
  125.6 8.9 %collective-permute-start.36 = (bf16[64,1024]{1,0:T(8,128)(2,1)S(1)}, bf16[64,1024]{1,0:T(8,128)(2,1)S(1)}, u32[]{:S(2)}, u32[]{:S(2)}) collective-permute-start(bf16[64,1024]{1,0:T(8,128)(2,1)S(1)} %get-tuple-element.66), channel_id=1, source_target_pairs={{0,32},{1,5},{2,34},{3,7},{4,36},{5,9},{6,38},{7,11},{8,40},{9,13}... | collective-permute-start | bytes 393224 | tf_op jit(solution)/shard_map/ppermute | solution.py:37
  (16 other events, 95.1 us)

commit v4 on v3

--- a/solution.py
+++ b/solution.py
@@ -183,24 +183,21 @@
             ] = fdot(rows, weight_ref[pl.ds(start, half), :])
 
 
-def early_kernel(lane_ref, *refs):
-    own, partner = refs[:EARLY], refs[EARLY : 2 * EARLY]
-    weights, own_out, partner_out = refs[2 * EARLY : -2], refs[-2], refs[-1]
-    half = own[0].shape[1]
-    project(own, weights, pl.multiple_of(lane_ref[0] * half, half), own_out, 0)
-    project(partner, weights, pl.multiple_of((1 - lane_ref[0]) * half, half), partner_out, 0)
+def half_kernel(partner, lane_ref, *refs):
+    chunks, weights, out_ref = refs[:-3], refs[-3:-1], refs[-1]
+    half = chunks[0].shape[1]
+    lane = 1 - lane_ref[0] if partner else lane_ref[0]
+    project(chunks, weights, pl.multiple_of(lane * half, half), out_ref, 0)
 
 
 def late_kernel(capacity, lane_ref, *refs):
     side = EXP_GRP
     late = side - EARLY
-    own, partner = refs[:late], refs[late : 2 * late]
-    weights, own_early, partner_early = refs[2 * late : -7], refs[-7], refs[-6]
-    mine_ref, own_late, partner_late = refs[-5], refs[-2], refs[-1]
-    theirs_refs = refs[-4:-2]
-    chunk, half = own[0].shape
+    partner, weights = refs[:late], refs[late : late + 2]
+    own_early, partner_early, own_late, mine_ref = refs[late + 2 : late + 6]
+    theirs_refs, partner_late = refs[late + 6 : late + 8], refs[late + 8]
+    chunk, half = partner[0].shape
     hidden = mine_ref.shape[1]
-    project(own, weights, pl.multiple_of(lane_ref[0] * half, half), own_late, 0)
     project(partner, weights, pl.multiple_of((1 - lane_ref[0]) * half, half), partner_late, 0)
     rows = ((0, EARLY, own_early), (EARLY, late, own_late))
     cols = ((0, EARLY, partner_early, theirs_refs[0]), (EARLY, late, partner_late, theirs_refs[1]))
@@ -318,11 +315,21 @@
     partner = []
     for delta, rows in zip(order, own):
         partner.append(lax.ppermute(rows, "tp", swap))
-    sums = ((EARLY * chunk, 2 * hidden_width), jnp.float32)
-    early = call(
-        early_kernel, [sums] * 2, lane, *own[:EARLY], *partner[:EARLY], *weights, scalars=1
-    )
     late = side - EARLY
+
+    def products(chunks, other):
+        return call(
+            functools.partial(half_kernel, other),
+            [((len(chunks) * chunk, 2 * hidden_width), jnp.float32)],
+            lane,
+            *chunks,
+            *weights,
+            scalars=1,
+        )[0]
+
+    own_early = products(own[:EARLY], False)
+    partner_early = products(partner[:EARLY], True)
+    own_late = products(own[EARLY:], False)
     mine, *theirs = call(
         functools.partial(late_kernel, capacity),
         [
@@ -331,18 +338,19 @@
             ((late * chunk, hidden_width), half_type),
         ],
         lane,
-        *own[EARLY:],
         *partner[EARLY:],
         *weights,
-        *early,
+        own_early,
+        partner_early,
+        own_late,
         scalars=1,
-        scratch=[pltpu.VMEM((late * chunk, 2 * hidden_width), jnp.float32)] * 2,
+        scratch=[pltpu.VMEM((late * chunk, 2 * hidden_width), jnp.float32)],
         limit=16,
     )
     near = lax.ppermute(theirs[0], "tp", swap)
     far = lax.ppermute(theirs[1], "tp", swap)
     returned = [None] * side
-    for some in (tuple(range(1, EARLY)), tuple(range(EARLY, side)) + (0,)):
+    for some in ((1,), tuple(range(2, EARLY)), tuple(range(EARLY, side)) + (0,)):
         results = call(
             functools.partial(down_kernel, some),
             [((chunk, part_width), half_type)] * len(some),

time: 137 us -> 138 us (level)
  waiting for transfers between devices: 34.6 us -> 44.1 us
  starting transfers between devices: 87.7 us -> 78.8 us
    ppermute x28, starting transfers between devices: 85.5 us -> 75.6 us  [shift(): return lax.ppermute(array, AXES, shift_pairs(gathering, delta))]
    ppermute x28, waiting for transfers between devices: 33.2 us -> 42.2 us  [shift(): return lax.ppermute(array, AXES, shift_pairs(gathering, delta))]
    pallas_call x8 -> x11, Pallas kernels: 13.7 us -> 14.1 us  [call(): pl.pallas_call(kernel, out_shape=[jax.ShapeDtypeStruct(*output) for outpu...]
  transfers between devices with their start and end apart: 39 -> 39, of which waited for: 16 -> 19; matrix products, arithmetic and copies ran while one was open for 0% -> 0% of each run, Pallas kernels for 9% -> 10%
where the time goes in v4:
time: 138 us
  starting transfers between devices  78.8 us (57%)
  waiting for transfers between devices  44.1 us (32%)
  Pallas kernels  14.1 us (10%)
    ppermute x28, starting transfers between devices, shift(): return lax.ppermute(array, AXES, shift_pairs(gathering, delta))  75.6 us
    ppermute x28, waiting for transfers between devices, shift(): return lax.ppermute(array, AXES, shift_pairs(gathering, delta))  42.2 us
    pallas_call x11, Pallas kernels, call(): pl.pallas_call(kernel, out_shape=[jax.ShapeDtypeStruct(*output) for outpu...  14.1 us
  transfers between devices with their start and end apart: 39, of which 19 were waited for; matrix products, arithmetic and copies ran while one was open for 0% of the time, Pallas kernels for 10%

profile of v4, /device:TPU:514, one launch (start us, length us, event | category | flops | bytes accessed | tf_op | source)
XLA Modules:
  0.0 138.0 jit_solution(154036733909613804)
XLA Ops:
  1.2 10.7 %collective-permute-start = (bf16[72,1024]{1,0:T(8,128)(2,1)S(1)}, bf16[72,1024]{1,0:T(8,128)(2,1)S(1)}, u32[]{:S(2)}, u32[]{:S(2)}) collective-permute-start(bf16[72,1024]{1,0:T(8,128)(2,1)S(1)} %shard_map.82.refs_0_), channel_id=1, source_target_pairs={{0,64},{1,9},{2,66},{3,11},{4,68},{5,13},{6,70},{7,15},{8,72},{9,1... | collective-permute-start | bytes 442376 | tf_op jit(solution)/shard_map/ppermute | solution.py:37
  11.9 4.5 %collective-permute-start.1 = (bf16[72,1024]{1,0:T(8,128)(2,1)S(1)}, bf16[72,1024]{1,0:T(8,128)(2,1)S(1)}, u32[]{:S(2)}, u32[]{:S(2)}) collective-permute-start(bf16[72,1024]{1,0:T(8,128)(2,1)S(1)} %shard_map.82.refs_0_), channel_id=1, source_target_pairs={{0,48},{1,7},{2,50},{3,9},{4,52},{5,11},{6,54},{7,13},{8,56},{9,15... | collective-permute-start | bytes 442376 | tf_op jit(solution)/shard_map/ppermute | solution.py:37
  16.9 3.2 %collective-permute-start.3 = (bf16[72,1024]{1,0:T(8,128)(2,1)S(1)}, bf16[72,1024]{1,0:T(8,128)(2,1)S(1)}, u32[]{:S(2)}, u32[]{:S(2)}) collective-permute-start(bf16[72,1024]{1,0:T(8,128)(2,1)S(1)} %shard_map.82.refs_0_), channel_id=1, source_target_pairs={{0,32},{1,5},{2,34},{3,7},{4,36},{5,9},{6,38},{7,11},{8,40},{9,13}... | collective-permute-start | bytes 442376 | tf_op jit(solution)/shard_map/ppermute | solution.py:37
  24.1 3.7 %collective-permute-start.6 = (bf16[72,1024]{1,0:T(8,128)(2,1)S(1)}, bf16[72,1024]{1,0:T(8,128)(2,1)S(1)}, u32[]{:S(2)}, u32[]{:S(2)}) collective-permute-start(bf16[72,1024]{1,0:T(8,128)(2,1)S(1)} %shard_map.82.refs_0_), channel_id=1, source_target_pairs={{0,112},{1,15},{2,114},{3,1},{4,116},{5,3},{6,118},{7,5},{8,120},{... | collective-permute-start | bytes 442376 | tf_op jit(solution)/shard_map/ppermute | solution.py:37
  29.3 2.2 %collective-permute-done.6.refs_7_ = bf16[72,1024]{1,0:T(8,128)(2,1)S(1)} collective-permute-done((bf16[72,1024]{1,0:T(8,128)(2,1)S(1)}, bf16[72,1024]{1,0:T(8,128)(2,1)S(1)}, u32[]{:S(2)}, u32[]{:S(2)}) %collective-permute-start.6) | collective-permute-done | bytes 147488 | tf_op jit(solution)/shard_map/ppermute | solution.py:37
  34.2 7.1 %collective-permute-start.13 = (bf16[128,1024]{1,0:T(8,128)(2,1)S(1)}, bf16[128,1024]{1,0:T(8,128)(2,1)S(1)}, u32[]{:S(2)}, u32[]{:S(2)}) collective-permute-start(bf16[128,1024]{1,0:T(8,128)(2,1)S(1)} %get-tuple-element.37), channel_id=1, source_target_pairs={{0,14},{1,113},{2,0},{3,115},{4,2},{5,117},{6,4},{7,119},{8,6},{9,... | collective-permute-start | bytes 786440 | tf_op jit(solution)/shard_map/ppermute | solution.py:37
  41.3 4.1 %collective-permute-start.9 = (bf16[128,1024]{1,0:T(8,128)(2,1)S(1)}, bf16[128,1024]{1,0:T(8,128)(2,1)S(1)}, u32[]{:S(2)}, u32[]{:S(2)}) collective-permute-start(bf16[128,1024]{1,0:T(8,128)(2,1)S(1)} %get-tuple-element.35), channel_id=1, source_target_pairs={{0,12},{1,97},{2,14},{3,99},{4,0},{5,101},{6,2},{7,103},{8,4},{9,1... | collective-permute-start | bytes 786440 | tf_op jit(solution)/shard_map/ppermute | solution.py:37
  46.2 7.0 %collective-permute-start.16 = (bf16[128,1024]{1,0:T(8,128)(2,1)S(1)}, bf16[128,1024]{1,0:T(8,128)(2,1)S(1)}, u32[]{:S(2)}, u32[]{:S(2)}) collective-permute-start(bf16[128,1024]{1,0:T(8,128)(2,1)S(1)} %get-tuple-element.42), channel_id=1, source_target_pairs={{0,6},{1,49},{2,8},{3,51},{4,10},{5,53},{6,12},{7,55},{8,14},{9,57... | collective-permute-start | bytes 786440 | tf_op jit(solution)/shard_map/ppermute | solution.py:37
  53.2 10.3 %collective-permute-done.7.refs_0_ = bf16[128,1024]{1,0:T(8,128)(2,1)S(1)} collective-permute-done((bf16[128,1024]{1,0:T(8,128)(2,1)S(1)}, bf16[128,1024]{1,0:T(8,128)(2,1)S(1)}, u32[]{:S(2)}, u32[]{:S(2)}) %collective-permute-start.7) | collective-permute-done | bytes 262176 | tf_op jit(solution)/shard_map/ppermute | solution.py:37
  65.5 7.3 %collective-permute-done.17.refs_3_ = bf16[128,1024]{1,0:T(8,128)(2,1)S(1)} collective-permute-done((bf16[128,1024]{1,0:T(8,128)(2,1)S(1)}, bf16[128,1024]{1,0:T(8,128)(2,1)S(1)}, u32[]{:S(2)}, u32[]{:S(2)}) %collective-permute-start.17) | collective-permute-done | bytes 262176 | tf_op jit(solution)/shard_map/ppermute | solution.py:37
  74.5 2.3 %shard_map.84 = (bf16[8,128,128]{2,1,0:T(8,128)(2,1)S(1)}, bf16[2048,512]{1,0:T(8,128)(2,1)S(1)}, bf16[2048,512]{1,0:T(8,128)(2,1)S(1)}) custom-call(s32[1]{0:T(128)} %bitcast.lane_ref, s32[1]{0:T(128)} %bitcast.1.place_ref, bf16[72,1024]{1,0:T(8,128)(2,1)S(1)} %shard_map.82.refs_0_, bf16[72,1024]{1,0:T(8,128)(2,1)S(1)} %collective-permute-done.refs_1_, ...), custom_call_target="tpu_custom_call" | custom-call | tf_op jit(solution)/shard_map/pallas_call | solution.py:48
  80.7 2.6 %shard_map.88 = (bf16[1024,512]{1,0:T(8,128)(2,1)S(1)}, bf16[512,512]{1,0:T(8,128)(2,1)S(1)}, bf16[512,512]{1,0:T(8,128)(2,1)S(1)}) custom-call(s32[1]{0:T(128)} %bitcast.lane_ref, bf16[128,1024]{1,0:T(8,128)(2,1)S(1)} %collective-permute-done.8.refs_0_, bf16[128,1024]{1,0:T(8,128)(2,1)S(1)} %collective-permute-done.10.refs_1_, ...), custom_call_target="tpu_custom_call" | custom-call | tf_op jit(solution)/shard_map/pallas_call | solution.py:48
  86.0 2.9 %collective-permute-start.26 = (bf16[128,1024]{1,0:T(8,128)(2,1)S(1)}, bf16[128,1024]{1,0:T(8,128)(2,1)S(1)}, u32[]{:S(2)}, u32[]{:S(2)}) collective-permute-start(bf16[128,1024]{1,0:T(8,128)(2,1)S(1)} %get-tuple-element.48), channel_id=1, source_target_pairs={{0,10},{1,81},{2,12},{3,83},{4,14},{5,85},{6,0},{7,87},{8,2},{9,89... | collective-permute-start | bytes 786440 | tf_op jit(solution)/shard_map/ppermute | solution.py:37
  93.6 3.0 %collective-permute-start.28 = (bf16[128,1024]{1,0:T(8,128)(2,1)S(1)}, bf16[128,1024]{1,0:T(8,128)(2,1)S(1)}, u32[]{:S(2)}, u32[]{:S(2)}) collective-permute-start(bf16[128,1024]{1,0:T(8,128)(2,1)S(1)} %get-tuple-element.50), channel_id=1, source_target_pairs={{0,12},{1,97},{2,14},{3,99},{4,0},{5,101},{6,2},{7,103},{8,4},{9,1... | collective-permute-start | bytes 786440 | tf_op jit(solution)/shard_map/ppermute | solution.py:37
  99.6 2.7 %collective-permute-start.31 = (bf16[128,1024]{1,0:T(8,128)(2,1)S(1)}, bf16[128,1024]{1,0:T(8,128)(2,1)S(1)}, u32[]{:S(2)}, u32[]{:S(2)}) collective-permute-start(bf16[128,1024]{1,0:T(8,128)(2,1)S(1)} %get-tuple-element.53), channel_id=1, source_target_pairs={{0,2},{1,17},{2,4},{3,19},{4,6},{5,21},{6,8},{7,23},{8,10},{9,25},... | collective-permute-start | bytes 786440 | tf_op jit(solution)/shard_map/ppermute | solution.py:37
  102.2 4.0 %collective-permute-done.25.refs_1_ = bf16[128,1024]{1,0:T(8,128)(2,1)S(1)} collective-permute-done((bf16[128,1024]{1,0:T(8,128)(2,1)S(1)}, bf16[128,1024]{1,0:T(8,128)(2,1)S(1)}, u32[]{:S(2)}, u32[]{:S(2)}) %collective-permute-start.25) | collective-permute-done | bytes 262176 | tf_op jit(solution)/shard_map/ppermute | solution.py:37
  106.3 4.6 %collective-permute-done.29.refs_5_ = bf16[128,1024]{1,0:T(8,128)(2,1)S(1)} collective-permute-done((bf16[128,1024]{1,0:T(8,128)(2,1)S(1)}, bf16[128,1024]{1,0:T(8,128)(2,1)S(1)}, u32[]{:S(2)}, u32[]{:S(2)}) %collective-permute-start.29) | collective-permute-done | bytes 262176 | tf_op jit(solution)/shard_map/ppermute | solution.py:37
  110.9 2.5 %collective-permute-done.31.refs_7_ = bf16[128,1024]{1,0:T(8,128)(2,1)S(1)} collective-permute-done((bf16[128,1024]{1,0:T(8,128)(2,1)S(1)}, bf16[128,1024]{1,0:T(8,128)(2,1)S(1)}, u32[]{:S(2)}, u32[]{:S(2)}) %collective-permute-start.31) | collective-permute-done | bytes 262176 | tf_op jit(solution)/shard_map/ppermute | solution.py:37
  114.1 7.1 %collective-permute-start.32 = (bf16[64,1024]{1,0:T(8,128)(2,1)S(1)}, bf16[64,1024]{1,0:T(8,128)(2,1)S(1)}, u32[]{:S(2)}, u32[]{:S(2)}) collective-permute-start(bf16[64,1024]{1,0:T(8,128)(2,1)S(1)} %get-tuple-element.56), channel_id=1, source_target_pairs={{0,64},{1,9},{2,66},{3,11},{4,68},{5,13},{6,70},{7,15},{8,72},{9,1... | collective-permute-start | bytes 393224 | tf_op jit(solution)/shard_map/ppermute | solution.py:37
  121.3 3.8 %collective-permute-start.34 = (bf16[64,1024]{1,0:T(8,128)(2,1)S(1)}, bf16[64,1024]{1,0:T(8,128)(2,1)S(1)}, u32[]{:S(2)}, u32[]{:S(2)}) collective-permute-start(bf16[64,1024]{1,0:T(8,128)(2,1)S(1)} %get-tuple-element.58), channel_id=1, source_target_pairs={{0,48},{1,7},{2,50},{3,9},{4,52},{5,11},{6,54},{7,13},{8,56},{9,15... | collective-permute-start | bytes 393224 | tf_op jit(solution)/shard_map/ppermute | solution.py:37
  125.6 2.5 %collective-permute-start.36 = (bf16[64,1024]{1,0:T(8,128)(2,1)S(1)}, bf16[64,1024]{1,0:T(8,128)(2,1)S(1)}, u32[]{:S(2)}, u32[]{:S(2)}) collective-permute-start(bf16[64,1024]{1,0:T(8,128)(2,1)S(1)} %get-tuple-element.60), channel_id=1, source_target_pairs={{0,32},{1,5},{2,34},{3,7},{4,36},{5,9},{6,38},{7,11},{8,40},{9,13}... | collective-permute-start | bytes 393224 | tf_op jit(solution)/shard_map/ppermute | solution.py:37
  128.0 2.9 %collective-permute-start.37 = (bf16[64,1024]{1,0:T(8,128)(2,1)S(1)}, bf16[64,1024]{1,0:T(8,128)(2,1)S(1)}, u32[]{:S(2)}, u32[]{:S(2)}) collective-permute-start(bf16[64,1024]{1,0:T(8,128)(2,1)S(1)} %get-tuple-element.61), channel_id=1, source_target_pairs={{0,112},{1,15},{2,114},{3,1},{4,116},{5,3},{6,118},{7,5},{8,120},{... | collective-permute-start | bytes 393224 | tf_op jit(solution)/shard_map/ppermute | solution.py:37
  131.1 2.6 %collective-permute-done.36 = bf16[64,1024]{1,0:T(8,128)(2,1)S(1)} collective-permute-done((bf16[64,1024]{1,0:T(8,128)(2,1)S(1)}, bf16[64,1024]{1,0:T(8,128)(2,1)S(1)}, u32[]{:S(2)}, u32[]{:S(2)}) %collective-permute-start.36) | collective-permute-done | bytes 131104 | tf_op jit(solution)/shard_map/ppermute | solution.py:37
  133.8 3.4 %collective-permute-done.38 = bf16[64,1024]{1,0:T(8,128)(2,1)S(1)} collective-permute-done((bf16[64,1024]{1,0:T(8,128)(2,1)S(1)}, bf16[64,1024]{1,0:T(8,128)(2,1)S(1)}, u32[]{:S(2)}, u32[]{:S(2)}) %collective-permute-start.38) | collective-permute-done | bytes 131104 | tf_op jit(solution)/shard_map/ppermute | solution.py:37
  (68 shorter events, 30.5 us)
Async XLA Ops:
  0.0 85.3 %collective-permute-start.24 = (bf16[512,2048]{1,0:T(8,128)(2,1)}, bf16[512,2048]{1,0:T(8,128)(2,1)S(1)}, u32[]{:S(2)}, u32[]{:S(2)}) collective-permute-start(bf16[512,2048]{1,0:T(8,128)(2,1)} %bitcast.9), channel_id=1, source_target_pairs={{0,1},{1,0},{2,3},{3,2},{4,5},{5,4},{6,7},{7,6},{8,9},{9,8},{10,11... | collective-permute-start | bytes 6291464 | tf_op jit(solution)/shard_map/ppermute | solution.py:267
  1.2 19.0 %collective-permute-start = (bf16[72,1024]{1,0:T(8,128)(2,1)S(1)}, bf16[72,1024]{1,0:T(8,128)(2,1)S(1)}, u32[]{:S(2)}, u32[]{:S(2)}) collective-permute-start(bf16[72,1024]{1,0:T(8,128)(2,1)S(1)} %shard_map.82.refs_0_), channel_id=1, source_target_pairs={{0,64},{1,9},{2,66},{3,11},{4,68},{5,13},{6,70},{7,15},{8,72},{9,1... | collective-permute-start | bytes 442376 | tf_op jit(solution)/shard_map/ppermute | solution.py:37
  11.9 11.1 %collective-permute-start.1 = (bf16[72,1024]{1,0:T(8,128)(2,1)S(1)}, bf16[72,1024]{1,0:T(8,128)(2,1)S(1)}, u32[]{:S(2)}, u32[]{:S(2)}) collective-permute-start(bf16[72,1024]{1,0:T(8,128)(2,1)S(1)} %shard_map.82.refs_0_), channel_id=1, source_target_pairs={{0,48},{1,7},{2,50},{3,9},{4,52},{5,11},{6,54},{7,13},{8,56},{9,15... | collective-permute-start | bytes 442376 | tf_op jit(solution)/shard_map/ppermute | solution.py:37
  16.9 10.8 %collective-permute-start.3 = (bf16[72,1024]{1,0:T(8,128)(2,1)S(1)}, bf16[72,1024]{1,0:T(8,128)(2,1)S(1)}, u32[]{:S(2)}, u32[]{:S(2)}) collective-permute-start(bf16[72,1024]{1,0:T(8,128)(2,1)S(1)} %shard_map.82.refs_0_), channel_id=1, source_target_pairs={{0,32},{1,5},{2,34},{3,7},{4,36},{5,9},{6,38},{7,11},{8,40},{9,13}... | collective-permute-start | bytes 442376 | tf_op jit(solution)/shard_map/ppermute | solution.py:37
  32.4 13.1 %collective-permute-start.11 = (bf16[128,1024]{1,0:T(8,128)(2,1)S(1)}, bf16[128,1024]{1,0:T(8,128)(2,1)S(1)}, u32[]{:S(2)}, u32[]{:S(2)}) collective-permute-start(bf16[128,1024]{1,0:T(8,128)(2,1)S(1)} %get-tuple-element.36), channel_id=1, source_target_pairs={{0,2},{1,17},{2,4},{3,19},{4,6},{5,21},{6,8},{7,23},{8,10},{9,25},... | collective-permute-start | bytes 786440 | tf_op jit(solution)/shard_map/ppermute | solution.py:37
  34.2 12.0 %collective-permute-start.13 = (bf16[128,1024]{1,0:T(8,128)(2,1)S(1)}, bf16[128,1024]{1,0:T(8,128)(2,1)S(1)}, u32[]{:S(2)}, u32[]{:S(2)}) collective-permute-start(bf16[128,1024]{1,0:T(8,128)(2,1)S(1)} %get-tuple-element.37), channel_id=1, source_target_pairs={{0,14},{1,113},{2,0},{3,115},{4,2},{5,117},{6,4},{7,119},{8,6},{9,... | collective-permute-start | bytes 786440 | tf_op jit(solution)/shard_map/ppermute | solution.py:37
  41.3 22.2 %collective-permute-start.7 = (bf16[128,1024]{1,0:T(8,128)(2,1)S(1)}, bf16[128,1024]{1,0:T(8,128)(2,1)S(1)}, u32[]{:S(2)}, u32[]{:S(2)}) collective-permute-start(bf16[128,1024]{1,0:T(8,128)(2,1)S(1)} %get-tuple-element.34), channel_id=1, source_target_pairs={{0,4},{1,33},{2,6},{3,35},{4,8},{5,37},{6,10},{7,39},{8,12},{9,41}... | collective-permute-start | bytes 786440 | tf_op jit(solution)/shard_map/ppermute | solution.py:37
  41.3 22.2 %collective-permute-start.9 = (bf16[128,1024]{1,0:T(8,128)(2,1)S(1)}, bf16[128,1024]{1,0:T(8,128)(2,1)S(1)}, u32[]{:S(2)}, u32[]{:S(2)}) collective-permute-start(bf16[128,1024]{1,0:T(8,128)(2,1)S(1)} %get-tuple-element.35), channel_id=1, source_target_pairs={{0,12},{1,97},{2,14},{3,99},{4,0},{5,101},{6,2},{7,103},{8,4},{9,1... | collective-permute-start | bytes 786440 | tf_op jit(solution)/shard_map/ppermute | solution.py:37
  45.5 18.6 %collective-permute-start.15 = (bf16[128,1024]{1,0:T(8,128)(2,1)S(1)}, bf16[128,1024]{1,0:T(8,128)(2,1)S(1)}, u32[]{:S(2)}, u32[]{:S(2)}) collective-permute-start(bf16[128,1024]{1,0:T(8,128)(2,1)S(1)} %get-tuple-element.41), channel_id=1, source_target_pairs={{0,8},{1,65},{2,10},{3,67},{4,12},{5,69},{6,14},{7,71},{8,0},{9,73... | collective-permute-start | bytes 786440 | tf_op jit(solution)/shard_map/ppermute | solution.py:37
  46.2 17.9 %collective-permute-start.16 = (bf16[128,1024]{1,0:T(8,128)(2,1)S(1)}, bf16[128,1024]{1,0:T(8,128)(2,1)S(1)}, u32[]{:S(2)}, u32[]{:S(2)}) collective-permute-start(bf16[128,1024]{1,0:T(8,128)(2,1)S(1)} %get-tuple-element.42), channel_id=1, source_target_pairs={{0,6},{1,49},{2,8},{3,51},{4,10},{5,53},{6,12},{7,55},{8,14},{9,57... | collective-permute-start | bytes 786440 | tf_op jit(solution)/shard_map/ppermute | solution.py:37
  63.4 9.4 %collective-permute-start.17 = (bf16[128,1024]{1,0:T(8,128)(2,1)S(1)}, bf16[128,1024]{1,0:T(8,128)(2,1)S(1)}, u32[]{:S(2)}, u32[]{:S(2)}) collective-permute-start(bf16[128,1024]{1,0:T(8,128)(2,1)S(1)} %get-tuple-element.43), channel_id=1, source_target_pairs={{0,10},{1,81},{2,12},{3,83},{4,14},{5,85},{6,0},{7,87},{8,2},{9,89... | collective-permute-start | bytes 786440 | tf_op jit(solution)/shard_map/ppermute | solution.py:37
  63.5 9.4 %collective-permute-start.18 = (bf16[128,1024]{1,0:T(8,128)(2,1)S(1)}, bf16[128,1024]{1,0:T(8,128)(2,1)S(1)}, u32[]{:S(2)}, u32[]{:S(2)}) collective-permute-start(bf16[128,1024]{1,0:T(8,128)(2,1)S(1)} %get-tuple-element.40.refs_0_), channel_id=1, source_target_pairs={{0,1},{1,0},{2,3},{3,2},{4,5},{5,4},{6,7},{7,6},{8,9},{9,8},{10,11... | collective-permute-start | bytes 786440 | tf_op jit(solution)/shard_map/ppermute | solution.py:317
  64.1 9.2 %collective-permute-start.19 = (bf16[128,1024]{1,0:T(8,128)(2,1)S(1)}, bf16[128,1024]{1,0:T(8,128)(2,1)S(1)}, u32[]{:S(2)}, u32[]{:S(2)}) collective-permute-start(bf16[128,1024]{1,0:T(8,128)(2,1)S(1)} %collective-permute-done.15.refs_1_), channel_id=1, source_target_pairs={{0,1},{1,0},{2,3},{3,2},{4,5},{5,4},{6,7},{7,6},{8,9},{9,8},{10,11... | collective-permute-start | bytes 786440 | tf_op jit(solution)/shard_map/ppermute | solution.py:317
  64.1 9.4 %collective-permute-start.20 = (bf16[128,1024]{1,0:T(8,128)(2,1)S(1)}, bf16[128,1024]{1,0:T(8,128)(2,1)S(1)}, u32[]{:S(2)}, u32[]{:S(2)}) collective-permute-start(bf16[128,1024]{1,0:T(8,128)(2,1)S(1)} %collective-permute-done.16.refs_2_), channel_id=1, source_target_pairs={{0,1},{1,0},{2,3},{3,2},{4,5},{5,4},{6,7},{7,6},{8,9},{9,8},{10,11... | collective-permute-start | bytes 786440 | tf_op jit(solution)/shard_map/ppermute | solution.py:317
  86.0 12.4 %collective-permute-start.26 = (bf16[128,1024]{1,0:T(8,128)(2,1)S(1)}, bf16[128,1024]{1,0:T(8,128)(2,1)S(1)}, u32[]{:S(2)}, u32[]{:S(2)}) collective-permute-start(bf16[128,1024]{1,0:T(8,128)(2,1)S(1)} %get-tuple-element.48), channel_id=1, source_target_pairs={{0,10},{1,81},{2,12},{3,83},{4,14},{5,85},{6,0},{7,87},{8,2},{9,89... | collective-permute-start | bytes 786440 | tf_op jit(solution)/shard_map/ppermute | solution.py:37
  89.0 10.6 %collective-permute-start.27 = (bf16[128,1024]{1,0:T(8,128)(2,1)S(1)}, bf16[128,1024]{1,0:T(8,128)(2,1)S(1)}, u32[]{:S(2)}, u32[]{:S(2)}) collective-permute-start(bf16[128,1024]{1,0:T(8,128)(2,1)S(1)} %get-tuple-element.49), channel_id=1, source_target_pairs={{0,6},{1,49},{2,8},{3,51},{4,10},{5,53},{6,12},{7,55},{8,14},{9,57... | collective-permute-start | bytes 786440 | tf_op jit(solution)/shard_map/ppermute | solution.py:37
  91.6 14.7 %collective-permute-start.25 = (bf16[128,1024]{1,0:T(8,128)(2,1)S(1)}, bf16[128,1024]{1,0:T(8,128)(2,1)S(1)}, u32[]{:S(2)}, u32[]{:S(2)}) collective-permute-start(bf16[128,1024]{1,0:T(8,128)(2,1)S(1)} %shard_map.90), channel_id=1, source_target_pairs={{0,8},{1,65},{2,10},{3,67},{4,12},{5,69},{6,14},{7,71},{8,0},{9,73... | collective-permute-start | bytes 786440 | tf_op jit(solution)/shard_map/ppermute | solution.py:37
  93.6 12.7 %collective-permute-start.28 = (bf16[128,1024]{1,0:T(8,128)(2,1)S(1)}, bf16[128,1024]{1,0:T(8,128)(2,1)S(1)}, u32[]{:S(2)}, u32[]{:S(2)}) collective-permute-start(bf16[128,1024]{1,0:T(8,128)(2,1)S(1)} %get-tuple-element.50), channel_id=1, source_target_pairs={{0,12},{1,97},{2,14},{3,99},{4,0},{5,101},{6,2},{7,103},{8,4},{9,1... | collective-permute-start | bytes 786440 | tf_op jit(solution)/shard_map/ppermute | solution.py:37
  96.6 14.3 %collective-permute-start.29 = (bf16[128,1024]{1,0:T(8,128)(2,1)S(1)}, bf16[128,1024]{1,0:T(8,128)(2,1)S(1)}, u32[]{:S(2)}, u32[]{:S(2)}) collective-permute-start(bf16[128,1024]{1,0:T(8,128)(2,1)S(1)} %get-tuple-element.51), channel_id=1, source_target_pairs={{0,4},{1,33},{2,6},{3,35},{4,8},{5,37},{6,10},{7,39},{8,12},{9,41}... | collective-permute-start | bytes 786440 | tf_op jit(solution)/shard_map/ppermute | solution.py:37
  98.4 12.5 %collective-permute-start.30 = (bf16[128,1024]{1,0:T(8,128)(2,1)S(1)}, bf16[128,1024]{1,0:T(8,128)(2,1)S(1)}, u32[]{:S(2)}, u32[]{:S(2)}) collective-permute-start(bf16[128,1024]{1,0:T(8,128)(2,1)S(1)} %get-tuple-element.52), channel_id=1, source_target_pairs={{0,14},{1,113},{2,0},{3,115},{4,2},{5,117},{6,4},{7,119},{8,6},{9,... | collective-permute-start | bytes 786440 | tf_op jit(solution)/shard_map/ppermute | solution.py:37
  99.6 13.8 %collective-permute-start.31 = (bf16[128,1024]{1,0:T(8,128)(2,1)S(1)}, bf16[128,1024]{1,0:T(8,128)(2,1)S(1)}, u32[]{:S(2)}, u32[]{:S(2)}) collective-permute-start(bf16[128,1024]{1,0:T(8,128)(2,1)S(1)} %get-tuple-element.53), channel_id=1, source_target_pairs={{0,2},{1,17},{2,4},{3,19},{4,6},{5,21},{6,8},{7,23},{8,10},{9,25},... | collective-permute-start | bytes 786440 | tf_op jit(solution)/shard_map/ppermute | solution.py:37
  114.1 13.9 %collective-permute-start.32 = (bf16[64,1024]{1,0:T(8,128)(2,1)S(1)}, bf16[64,1024]{1,0:T(8,128)(2,1)S(1)}, u32[]{:S(2)}, u32[]{:S(2)}) collective-permute-start(bf16[64,1024]{1,0:T(8,128)(2,1)S(1)} %get-tuple-element.56), channel_id=1, source_target_pairs={{0,64},{1,9},{2,66},{3,11},{4,68},{5,13},{6,70},{7,15},{8,72},{9,1... | collective-permute-start | bytes 393224 | tf_op jit(solution)/shard_map/ppermute | solution.py:37
  121.3 9.7 %collective-permute-start.33 = (bf16[64,1024]{1,0:T(8,128)(2,1)S(1)}, bf16[64,1024]{1,0:T(8,128)(2,1)S(1)}, u32[]{:S(2)}, u32[]{:S(2)}) collective-permute-start(bf16[64,1024]{1,0:T(8,128)(2,1)S(1)} %get-tuple-element.57), channel_id=1, source_target_pairs={{0,80},{1,11},{2,82},{3,13},{4,84},{5,15},{6,86},{7,1},{8,88},{9,3... | collective-permute-start | bytes 393224 | tf_op jit(solution)/shard_map/ppermute | solution.py:37
  121.3 9.7 %collective-permute-start.34 = (bf16[64,1024]{1,0:T(8,128)(2,1)S(1)}, bf16[64,1024]{1,0:T(8,128)(2,1)S(1)}, u32[]{:S(2)}, u32[]{:S(2)}) collective-permute-start(bf16[64,1024]{1,0:T(8,128)(2,1)S(1)} %get-tuple-element.58), channel_id=1, source_target_pairs={{0,48},{1,7},{2,50},{3,9},{4,52},{5,11},{6,54},{7,13},{8,56},{9,15... | collective-permute-start | bytes 393224 | tf_op jit(solution)/shard_map/ppermute | solution.py:37
  (16 other events, 100.7 us)

commit v5 on v4

--- a/solution.py
+++ b/solution.py
@@ -217,7 +217,7 @@
                 theirs_ref[pl.ds(right, capacity), :] = acts
                 return carry
 
-            lax.fori_loop(0, count * far_count, block, 0, unroll=2)
+            lax.fori_loop(0, count * far_count, block, 0, unroll=4)
 
 
 def down_kernel(places, lane_ref, mine_ref, near_ref, far_ref, down_ref, other_ref, *outs):
@@ -233,16 +233,16 @@
         ).astype(jnp.bfloat16)
 
 
-def combine_kernel(capacity, *refs):
+def combine_kernel(capacity, places, *refs):
     side = EXP_GRP
     chunks, factors_ref, outs = refs[:side], refs[side], refs[side + 1 :]
-    for source in range(side):
+    for source, out_ref in zip(places, outs):
         rows = jnp.concatenate(
             [chunk[source * capacity : (source + 1) * capacity, :] for chunk in chunks], axis=0
         )
         both = fdot(factors_ref[source], rows)
         tokens = both.shape[0] // 2
-        outs[source][...] = (both[:tokens] + both[tokens:]).astype(outs[source].dtype)
+        out_ref[...] = (both[:tokens] + both[tokens:]).astype(out_ref.dtype)
 
 
 def layer(
@@ -364,15 +364,18 @@
         )
         for place, result in zip(some, results):
             returned[place] = shift(result, False, -order[place]) if place else result
-    kept, *partials = call(
-        functools.partial(combine_kernel, capacity),
-        [((token_count, part_width), jnp.float32)]
-        + [((token_count, part_width), half_type)] * (side - 1),
-        *returned,
-        factors,
-    )
-    total = kept
-    for place, delta in enumerate(order[1:]):
+    partials = [None] * side
+    for some in ((1,), (0,) + tuple(range(2, side))):
+        sums = call(
+            functools.partial(combine_kernel, capacity, some),
+            [((token_count, part_width), half_type if place else jnp.float32) for place in some],
+            *returned,
+            factors,
+        )
+        for place, partial in zip(some, sums):
+            partials[place] = partial
+    total = partials[0]
+    for place, delta in enumerate(order[1:], 1):
         total += shift(partials[place], True, -delta).astype(jnp.float32)
     return total.astype(half_type)
 

time: 138 us -> 138 us (level)
    pallas_call x11 -> x12, Pallas kernels: 14.1 us -> 14 us  [call(): pl.pallas_call(kernel, out_shape=[jax.ShapeDtypeStruct(*output) for outpu...]
where the time goes in v5:
time: 138 us
  starting transfers between devices  78.9 us (57%)
  waiting for transfers between devices  44 us (32%)
  Pallas kernels  14 us (10%)
    ppermute x28, starting transfers between devices, shift(): return lax.ppermute(array, AXES, shift_pairs(gathering, delta))  75.7 us
    ppermute x28, waiting for transfers between devices, shift(): return lax.ppermute(array, AXES, shift_pairs(gathering, delta))  42.1 us
    pallas_call x12, Pallas kernels, call(): pl.pallas_call(kernel, out_shape=[jax.ShapeDtypeStruct(*output) for outpu...  14 us
  transfers between devices with their start and end apart: 39, of which 19 were waited for; matrix products, arithmetic and copies ran while one was open for 0% of the time, Pallas kernels for 10%

profile of v5, /device:TPU:514, one launch (start us, length us, event | category | flops | bytes accessed | tf_op | source)
XLA Modules:
  0.0 138.0 jit_solution(8623635204907786029)
XLA Ops:
  1.2 10.7 %collective-permute-start = (bf16[72,1024]{1,0:T(8,128)(2,1)S(1)}, bf16[72,1024]{1,0:T(8,128)(2,1)S(1)}, u32[]{:S(2)}, u32[]{:S(2)}) collective-permute-start(bf16[72,1024]{1,0:T(8,128)(2,1)S(1)} %shard_map.82.refs_0_), channel_id=1, source_target_pairs={{0,64},{1,9},{2,66},{3,11},{4,68},{5,13},{6,70},{7,15},{8,72},{9,1... | collective-permute-start | bytes 442376 | tf_op jit(solution)/shard_map/ppermute | solution.py:37
  11.9 4.5 %collective-permute-start.1 = (bf16[72,1024]{1,0:T(8,128)(2,1)S(1)}, bf16[72,1024]{1,0:T(8,128)(2,1)S(1)}, u32[]{:S(2)}, u32[]{:S(2)}) collective-permute-start(bf16[72,1024]{1,0:T(8,128)(2,1)S(1)} %shard_map.82.refs_0_), channel_id=1, source_target_pairs={{0,48},{1,7},{2,50},{3,9},{4,52},{5,11},{6,54},{7,13},{8,56},{9,15... | collective-permute-start | bytes 442376 | tf_op jit(solution)/shard_map/ppermute | solution.py:37
  16.9 3.2 %collective-permute-start.3 = (bf16[72,1024]{1,0:T(8,128)(2,1)S(1)}, bf16[72,1024]{1,0:T(8,128)(2,1)S(1)}, u32[]{:S(2)}, u32[]{:S(2)}) collective-permute-start(bf16[72,1024]{1,0:T(8,128)(2,1)S(1)} %shard_map.82.refs_0_), channel_id=1, source_target_pairs={{0,32},{1,5},{2,34},{3,7},{4,36},{5,9},{6,38},{7,11},{8,40},{9,13}... | collective-permute-start | bytes 442376 | tf_op jit(solution)/shard_map/ppermute | solution.py:37
  24.1 3.7 %collective-permute-start.6 = (bf16[72,1024]{1,0:T(8,128)(2,1)S(1)}, bf16[72,1024]{1,0:T(8,128)(2,1)S(1)}, u32[]{:S(2)}, u32[]{:S(2)}) collective-permute-start(bf16[72,1024]{1,0:T(8,128)(2,1)S(1)} %shard_map.82.refs_0_), channel_id=1, source_target_pairs={{0,112},{1,15},{2,114},{3,1},{4,116},{5,3},{6,118},{7,5},{8,120},{... | collective-permute-start | bytes 442376 | tf_op jit(solution)/shard_map/ppermute | solution.py:37
  29.3 2.2 %collective-permute-done.6.refs_7_ = bf16[72,1024]{1,0:T(8,128)(2,1)S(1)} collective-permute-done((bf16[72,1024]{1,0:T(8,128)(2,1)S(1)}, bf16[72,1024]{1,0:T(8,128)(2,1)S(1)}, u32[]{:S(2)}, u32[]{:S(2)}) %collective-permute-start.6) | collective-permute-done | bytes 147488 | tf_op jit(solution)/shard_map/ppermute | solution.py:37
  34.2 7.1 %collective-permute-start.13 = (bf16[128,1024]{1,0:T(8,128)(2,1)S(1)}, bf16[128,1024]{1,0:T(8,128)(2,1)S(1)}, u32[]{:S(2)}, u32[]{:S(2)}) collective-permute-start(bf16[128,1024]{1,0:T(8,128)(2,1)S(1)} %get-tuple-element.36), channel_id=1, source_target_pairs={{0,14},{1,113},{2,0},{3,115},{4,2},{5,117},{6,4},{7,119},{8,6},{9,... | collective-permute-start | bytes 786440 | tf_op jit(solution)/shard_map/ppermute | solution.py:37
  41.3 4.1 %collective-permute-start.9 = (bf16[128,1024]{1,0:T(8,128)(2,1)S(1)}, bf16[128,1024]{1,0:T(8,128)(2,1)S(1)}, u32[]{:S(2)}, u32[]{:S(2)}) collective-permute-start(bf16[128,1024]{1,0:T(8,128)(2,1)S(1)} %get-tuple-element.34), channel_id=1, source_target_pairs={{0,12},{1,97},{2,14},{3,99},{4,0},{5,101},{6,2},{7,103},{8,4},{9,1... | collective-permute-start | bytes 786440 | tf_op jit(solution)/shard_map/ppermute | solution.py:37
  46.2 7.0 %collective-permute-start.16 = (bf16[128,1024]{1,0:T(8,128)(2,1)S(1)}, bf16[128,1024]{1,0:T(8,128)(2,1)S(1)}, u32[]{:S(2)}, u32[]{:S(2)}) collective-permute-start(bf16[128,1024]{1,0:T(8,128)(2,1)S(1)} %get-tuple-element.41), channel_id=1, source_target_pairs={{0,6},{1,49},{2,8},{3,51},{4,10},{5,53},{6,12},{7,55},{8,14},{9,57... | collective-permute-start | bytes 786440 | tf_op jit(solution)/shard_map/ppermute | solution.py:37
  53.2 10.3 %collective-permute-done.7.refs_0_ = bf16[128,1024]{1,0:T(8,128)(2,1)S(1)} collective-permute-done((bf16[128,1024]{1,0:T(8,128)(2,1)S(1)}, bf16[128,1024]{1,0:T(8,128)(2,1)S(1)}, u32[]{:S(2)}, u32[]{:S(2)}) %collective-permute-start.7) | collective-permute-done | bytes 262176 | tf_op jit(solution)/shard_map/ppermute | solution.py:37
  65.5 7.3 %collective-permute-done.17.refs_3_ = bf16[128,1024]{1,0:T(8,128)(2,1)S(1)} collective-permute-done((bf16[128,1024]{1,0:T(8,128)(2,1)S(1)}, bf16[128,1024]{1,0:T(8,128)(2,1)S(1)}, u32[]{:S(2)}, u32[]{:S(2)}) %collective-permute-start.17) | collective-permute-done | bytes 262176 | tf_op jit(solution)/shard_map/ppermute | solution.py:37
  74.5 2.3 %shard_map.84 = (bf16[8,128,128]{2,1,0:T(8,128)(2,1)S(1)}, bf16[2048,512]{1,0:T(8,128)(2,1)S(1)}, bf16[2048,512]{1,0:T(8,128)(2,1)S(1)}) custom-call(s32[1]{0:T(128)} %bitcast.lane_ref, s32[1]{0:T(128)} %bitcast.1.place_ref, bf16[72,1024]{1,0:T(8,128)(2,1)S(1)} %shard_map.82.refs_0_, bf16[72,1024]{1,0:T(8,128)(2,1)S(1)} %collective-permute-done.refs_1_, ...), custom_call_target="tpu_custom_call" | custom-call | tf_op jit(solution)/shard_map/pallas_call | solution.py:48
  80.7 2.3 %shard_map.88 = (bf16[1024,512]{1,0:T(8,128)(2,1)S(1)}, bf16[512,512]{1,0:T(8,128)(2,1)S(1)}, bf16[512,512]{1,0:T(8,128)(2,1)S(1)}) custom-call(s32[1]{0:T(128)} %bitcast.lane_ref, bf16[128,1024]{1,0:T(8,128)(2,1)S(1)} %collective-permute-done.8.refs_0_, bf16[128,1024]{1,0:T(8,128)(2,1)S(1)} %collective-permute-done.10.refs_1_, ...), custom_call_target="tpu_custom_call" | custom-call | tf_op jit(solution)/shard_map/pallas_call | solution.py:48
  85.7 2.9 %collective-permute-start.26 = (bf16[128,1024]{1,0:T(8,128)(2,1)S(1)}, bf16[128,1024]{1,0:T(8,128)(2,1)S(1)}, u32[]{:S(2)}, u32[]{:S(2)}) collective-permute-start(bf16[128,1024]{1,0:T(8,128)(2,1)S(1)} %get-tuple-element.47), channel_id=1, source_target_pairs={{0,10},{1,81},{2,12},{3,83},{4,14},{5,85},{6,0},{7,87},{8,2},{9,89... | collective-permute-start | bytes 786440 | tf_op jit(solution)/shard_map/ppermute | solution.py:37
  93.3 3.0 %collective-permute-start.28 = (bf16[128,1024]{1,0:T(8,128)(2,1)S(1)}, bf16[128,1024]{1,0:T(8,128)(2,1)S(1)}, u32[]{:S(2)}, u32[]{:S(2)}) collective-permute-start(bf16[128,1024]{1,0:T(8,128)(2,1)S(1)} %get-tuple-element.49), channel_id=1, source_target_pairs={{0,12},{1,97},{2,14},{3,99},{4,0},{5,101},{6,2},{7,103},{8,4},{9,1... | collective-permute-start | bytes 786440 | tf_op jit(solution)/shard_map/ppermute | solution.py:37
  99.3 2.7 %collective-permute-start.31 = (bf16[128,1024]{1,0:T(8,128)(2,1)S(1)}, bf16[128,1024]{1,0:T(8,128)(2,1)S(1)}, u32[]{:S(2)}, u32[]{:S(2)}) collective-permute-start(bf16[128,1024]{1,0:T(8,128)(2,1)S(1)} %get-tuple-element.52), channel_id=1, source_target_pairs={{0,2},{1,17},{2,4},{3,19},{4,6},{5,21},{6,8},{7,23},{8,10},{9,25},... | collective-permute-start | bytes 786440 | tf_op jit(solution)/shard_map/ppermute | solution.py:37
  102.0 4.1 %collective-permute-done.25.refs_1_ = bf16[128,1024]{1,0:T(8,128)(2,1)S(1)} collective-permute-done((bf16[128,1024]{1,0:T(8,128)(2,1)S(1)}, bf16[128,1024]{1,0:T(8,128)(2,1)S(1)}, u32[]{:S(2)}, u32[]{:S(2)}) %collective-permute-start.25) | collective-permute-done | bytes 262176 | tf_op jit(solution)/shard_map/ppermute | solution.py:37
  106.0 4.6 %collective-permute-done.29.refs_5_ = bf16[128,1024]{1,0:T(8,128)(2,1)S(1)} collective-permute-done((bf16[128,1024]{1,0:T(8,128)(2,1)S(1)}, bf16[128,1024]{1,0:T(8,128)(2,1)S(1)}, u32[]{:S(2)}, u32[]{:S(2)}) %collective-permute-start.29) | collective-permute-done | bytes 262176 | tf_op jit(solution)/shard_map/ppermute | solution.py:37
  110.6 2.5 %collective-permute-done.31.refs_7_ = bf16[128,1024]{1,0:T(8,128)(2,1)S(1)} collective-permute-done((bf16[128,1024]{1,0:T(8,128)(2,1)S(1)}, bf16[128,1024]{1,0:T(8,128)(2,1)S(1)}, u32[]{:S(2)}, u32[]{:S(2)}) %collective-permute-start.31) | collective-permute-done | bytes 262176 | tf_op jit(solution)/shard_map/ppermute | solution.py:37
  113.4 7.1 %collective-permute-start.32 = (bf16[64,1024]{1,0:T(8,128)(2,1)S(1)}, bf16[64,1024]{1,0:T(8,128)(2,1)S(1)}, u32[]{:S(2)}, u32[]{:S(2)}) collective-permute-start(bf16[64,1024]{1,0:T(8,128)(2,1)S(1)} %shard_map.93), channel_id=1, source_target_pairs={{0,64},{1,9},{2,66},{3,11},{4,68},{5,13},{6,70},{7,15},{8,72},{9,1... | collective-permute-start | bytes 393224 | tf_op jit(solution)/shard_map/ppermute | solution.py:37
  121.3 3.8 %collective-permute-start.34 = (bf16[64,1024]{1,0:T(8,128)(2,1)S(1)}, bf16[64,1024]{1,0:T(8,128)(2,1)S(1)}, u32[]{:S(2)}, u32[]{:S(2)}) collective-permute-start(bf16[64,1024]{1,0:T(8,128)(2,1)S(1)} %get-tuple-element.56), channel_id=1, source_target_pairs={{0,48},{1,7},{2,50},{3,9},{4,52},{5,11},{6,54},{7,13},{8,56},{9,15... | collective-permute-start | bytes 393224 | tf_op jit(solution)/shard_map/ppermute | solution.py:37
  125.5 2.5 %collective-permute-start.36 = (bf16[64,1024]{1,0:T(8,128)(2,1)S(1)}, bf16[64,1024]{1,0:T(8,128)(2,1)S(1)}, u32[]{:S(2)}, u32[]{:S(2)}) collective-permute-start(bf16[64,1024]{1,0:T(8,128)(2,1)S(1)} %get-tuple-element.58), channel_id=1, source_target_pairs={{0,32},{1,5},{2,34},{3,7},{4,36},{5,9},{6,38},{7,11},{8,40},{9,13}... | collective-permute-start | bytes 393224 | tf_op jit(solution)/shard_map/ppermute | solution.py:37
  128.0 3.0 %collective-permute-start.37 = (bf16[64,1024]{1,0:T(8,128)(2,1)S(1)}, bf16[64,1024]{1,0:T(8,128)(2,1)S(1)}, u32[]{:S(2)}, u32[]{:S(2)}) collective-permute-start(bf16[64,1024]{1,0:T(8,128)(2,1)S(1)} %get-tuple-element.59), channel_id=1, source_target_pairs={{0,112},{1,15},{2,114},{3,1},{4,116},{5,3},{6,118},{7,5},{8,120},{... | collective-permute-start | bytes 393224 | tf_op jit(solution)/shard_map/ppermute | solution.py:37
  131.4 2.4 %collective-permute-done.36 = bf16[64,1024]{1,0:T(8,128)(2,1)S(1)} collective-permute-done((bf16[64,1024]{1,0:T(8,128)(2,1)S(1)}, bf16[64,1024]{1,0:T(8,128)(2,1)S(1)}, u32[]{:S(2)}, u32[]{:S(2)}) %collective-permute-start.36) | collective-permute-done | bytes 131104 | tf_op jit(solution)/shard_map/ppermute | solution.py:37
  134.1 3.0 %collective-permute-done.38 = bf16[64,1024]{1,0:T(8,128)(2,1)S(1)} collective-permute-done((bf16[64,1024]{1,0:T(8,128)(2,1)S(1)}, bf16[64,1024]{1,0:T(8,128)(2,1)S(1)}, u32[]{:S(2)}, u32[]{:S(2)}) %collective-permute-start.38) | collective-permute-done | bytes 131104 | tf_op jit(solution)/shard_map/ppermute | solution.py:37
  (69 shorter events, 31.5 us)
Async XLA Ops:
  0.0 85.0 %collective-permute-start.24 = (bf16[512,2048]{1,0:T(8,128)(2,1)}, bf16[512,2048]{1,0:T(8,128)(2,1)S(1)}, u32[]{:S(2)}, u32[]{:S(2)}) collective-permute-start(bf16[512,2048]{1,0:T(8,128)(2,1)} %bitcast.9), channel_id=1, source_target_pairs={{0,1},{1,0},{2,3},{3,2},{4,5},{5,4},{6,7},{7,6},{8,9},{9,8},{10,11... | collective-permute-start | bytes 6291464 | tf_op jit(solution)/shard_map/ppermute | solution.py:267
  1.2 19.0 %collective-permute-start = (bf16[72,1024]{1,0:T(8,128)(2,1)S(1)}, bf16[72,1024]{1,0:T(8,128)(2,1)S(1)}, u32[]{:S(2)}, u32[]{:S(2)}) collective-permute-start(bf16[72,1024]{1,0:T(8,128)(2,1)S(1)} %shard_map.82.refs_0_), channel_id=1, source_target_pairs={{0,64},{1,9},{2,66},{3,11},{4,68},{5,13},{6,70},{7,15},{8,72},{9,1... | collective-permute-start | bytes 442376 | tf_op jit(solution)/shard_map/ppermute | solution.py:37
  11.9 11.1 %collective-permute-start.1 = (bf16[72,1024]{1,0:T(8,128)(2,1)S(1)}, bf16[72,1024]{1,0:T(8,128)(2,1)S(1)}, u32[]{:S(2)}, u32[]{:S(2)}) collective-permute-start(bf16[72,1024]{1,0:T(8,128)(2,1)S(1)} %shard_map.82.refs_0_), channel_id=1, source_target_pairs={{0,48},{1,7},{2,50},{3,9},{4,52},{5,11},{6,54},{7,13},{8,56},{9,15... | collective-permute-start | bytes 442376 | tf_op jit(solution)/shard_map/ppermute | solution.py:37
  16.9 10.8 %collective-permute-start.3 = (bf16[72,1024]{1,0:T(8,128)(2,1)S(1)}, bf16[72,1024]{1,0:T(8,128)(2,1)S(1)}, u32[]{:S(2)}, u32[]{:S(2)}) collective-permute-start(bf16[72,1024]{1,0:T(8,128)(2,1)S(1)} %shard_map.82.refs_0_), channel_id=1, source_target_pairs={{0,32},{1,5},{2,34},{3,7},{4,36},{5,9},{6,38},{7,11},{8,40},{9,13}... | collective-permute-start | bytes 442376 | tf_op jit(solution)/shard_map/ppermute | solution.py:37
  32.4 13.1 %collective-permute-start.11 = (bf16[128,1024]{1,0:T(8,128)(2,1)S(1)}, bf16[128,1024]{1,0:T(8,128)(2,1)S(1)}, u32[]{:S(2)}, u32[]{:S(2)}) collective-permute-start(bf16[128,1024]{1,0:T(8,128)(2,1)S(1)} %get-tuple-element.35), channel_id=1, source_target_pairs={{0,2},{1,17},{2,4},{3,19},{4,6},{5,21},{6,8},{7,23},{8,10},{9,25},... | collective-permute-start | bytes 786440 | tf_op jit(solution)/shard_map/ppermute | solution.py:37
  34.2 12.0 %collective-permute-start.13 = (bf16[128,1024]{1,0:T(8,128)(2,1)S(1)}, bf16[128,1024]{1,0:T(8,128)(2,1)S(1)}, u32[]{:S(2)}, u32[]{:S(2)}) collective-permute-start(bf16[128,1024]{1,0:T(8,128)(2,1)S(1)} %get-tuple-element.36), channel_id=1, source_target_pairs={{0,14},{1,113},{2,0},{3,115},{4,2},{5,117},{6,4},{7,119},{8,6},{9,... | collective-permute-start | bytes 786440 | tf_op jit(solution)/shard_map/ppermute | solution.py:37
  41.3 22.2 %collective-permute-start.7 = (bf16[128,1024]{1,0:T(8,128)(2,1)S(1)}, bf16[128,1024]{1,0:T(8,128)(2,1)S(1)}, u32[]{:S(2)}, u32[]{:S(2)}) collective-permute-start(bf16[128,1024]{1,0:T(8,128)(2,1)S(1)} %get-tuple-element.33), channel_id=1, source_target_pairs={{0,4},{1,33},{2,6},{3,35},{4,8},{5,37},{6,10},{7,39},{8,12},{9,41}... | collective-permute-start | bytes 786440 | tf_op jit(solution)/shard_map/ppermute | solution.py:37
  41.3 22.2 %collective-permute-start.9 = (bf16[128,1024]{1,0:T(8,128)(2,1)S(1)}, bf16[128,1024]{1,0:T(8,128)(2,1)S(1)}, u32[]{:S(2)}, u32[]{:S(2)}) collective-permute-start(bf16[128,1024]{1,0:T(8,128)(2,1)S(1)} %get-tuple-element.34), channel_id=1, source_target_pairs={{0,12},{1,97},{2,14},{3,99},{4,0},{5,101},{6,2},{7,103},{8,4},{9,1... | collective-permute-start | bytes 786440 | tf_op jit(solution)/shard_map/ppermute | solution.py:37
  45.5 18.6 %collective-permute-start.15 = (bf16[128,1024]{1,0:T(8,128)(2,1)S(1)}, bf16[128,1024]{1,0:T(8,128)(2,1)S(1)}, u32[]{:S(2)}, u32[]{:S(2)}) collective-permute-start(bf16[128,1024]{1,0:T(8,128)(2,1)S(1)} %get-tuple-element.40), channel_id=1, source_target_pairs={{0,8},{1,65},{2,10},{3,67},{4,12},{5,69},{6,14},{7,71},{8,0},{9,73... | collective-permute-start | bytes 786440 | tf_op jit(solution)/shard_map/ppermute | solution.py:37
  46.2 17.9 %collective-permute-start.16 = (bf16[128,1024]{1,0:T(8,128)(2,1)S(1)}, bf16[128,1024]{1,0:T(8,128)(2,1)S(1)}, u32[]{:S(2)}, u32[]{:S(2)}) collective-permute-start(bf16[128,1024]{1,0:T(8,128)(2,1)S(1)} %get-tuple-element.41), channel_id=1, source_target_pairs={{0,6},{1,49},{2,8},{3,51},{4,10},{5,53},{6,12},{7,55},{8,14},{9,57... | collective-permute-start | bytes 786440 | tf_op jit(solution)/shard_map/ppermute | solution.py:37
  63.4 9.4 %collective-permute-start.17 = (bf16[128,1024]{1,0:T(8,128)(2,1)S(1)}, bf16[128,1024]{1,0:T(8,128)(2,1)S(1)}, u32[]{:S(2)}, u32[]{:S(2)}) collective-permute-start(bf16[128,1024]{1,0:T(8,128)(2,1)S(1)} %get-tuple-element.42), channel_id=1, source_target_pairs={{0,10},{1,81},{2,12},{3,83},{4,14},{5,85},{6,0},{7,87},{8,2},{9,89... | collective-permute-start | bytes 786440 | tf_op jit(solution)/shard_map/ppermute | solution.py:37
  63.5 9.4 %collective-permute-start.18 = (bf16[128,1024]{1,0:T(8,128)(2,1)S(1)}, bf16[128,1024]{1,0:T(8,128)(2,1)S(1)}, u32[]{:S(2)}, u32[]{:S(2)}) collective-permute-start(bf16[128,1024]{1,0:T(8,128)(2,1)S(1)} %get-tuple-element.39.refs_0_), channel_id=1, source_target_pairs={{0,1},{1,0},{2,3},{3,2},{4,5},{5,4},{6,7},{7,6},{8,9},{9,8},{10,11... | collective-permute-start | bytes 786440 | tf_op jit(solution)/shard_map/ppermute | solution.py:317
  64.1 9.2 %collective-permute-start.19 = (bf16[128,1024]{1,0:T(8,128)(2,1)S(1)}, bf16[128,1024]{1,0:T(8,128)(2,1)S(1)}, u32[]{:S(2)}, u32[]{:S(2)}) collective-permute-start(bf16[128,1024]{1,0:T(8,128)(2,1)S(1)} %collective-permute-done.15.refs_1_), channel_id=1, source_target_pairs={{0,1},{1,0},{2,3},{3,2},{4,5},{5,4},{6,7},{7,6},{8,9},{9,8},{10,11... | collective-permute-start | bytes 786440 | tf_op jit(solution)/shard_map/ppermute | solution.py:317
  64.1 9.4 %collective-permute-start.20 = (bf16[128,1024]{1,0:T(8,128)(2,1)S(1)}, bf16[128,1024]{1,0:T(8,128)(2,1)S(1)}, u32[]{:S(2)}, u32[]{:S(2)}) collective-permute-start(bf16[128,1024]{1,0:T(8,128)(2,1)S(1)} %collective-permute-done.16.refs_2_), channel_id=1, source_target_pairs={{0,1},{1,0},{2,3},{3,2},{4,5},{5,4},{6,7},{7,6},{8,9},{9,8},{10,11... | collective-permute-start | bytes 786440 | tf_op jit(solution)/shard_map/ppermute | solution.py:317
  85.7 12.4 %collective-permute-start.26 = (bf16[128,1024]{1,0:T(8,128)(2,1)S(1)}, bf16[128,1024]{1,0:T(8,128)(2,1)S(1)}, u32[]{:S(2)}, u32[]{:S(2)}) collective-permute-start(bf16[128,1024]{1,0:T(8,128)(2,1)S(1)} %get-tuple-element.47), channel_id=1, source_target_pairs={{0,10},{1,81},{2,12},{3,83},{4,14},{5,85},{6,0},{7,87},{8,2},{9,89... | collective-permute-start | bytes 786440 | tf_op jit(solution)/shard_map/ppermute | solution.py:37
  88.7 10.6 %collective-permute-start.27 = (bf16[128,1024]{1,0:T(8,128)(2,1)S(1)}, bf16[128,1024]{1,0:T(8,128)(2,1)S(1)}, u32[]{:S(2)}, u32[]{:S(2)}) collective-permute-start(bf16[128,1024]{1,0:T(8,128)(2,1)S(1)} %get-tuple-element.48), channel_id=1, source_target_pairs={{0,6},{1,49},{2,8},{3,51},{4,10},{5,53},{6,12},{7,55},{8,14},{9,57... | collective-permute-start | bytes 786440 | tf_op jit(solution)/shard_map/ppermute | solution.py:37
  91.4 14.7 %collective-permute-start.25 = (bf16[128,1024]{1,0:T(8,128)(2,1)S(1)}, bf16[128,1024]{1,0:T(8,128)(2,1)S(1)}, u32[]{:S(2)}, u32[]{:S(2)}) collective-permute-start(bf16[128,1024]{1,0:T(8,128)(2,1)S(1)} %shard_map.90), channel_id=1, source_target_pairs={{0,8},{1,65},{2,10},{3,67},{4,12},{5,69},{6,14},{7,71},{8,0},{9,73... | collective-permute-start | bytes 786440 | tf_op jit(solution)/shard_map/ppermute | solution.py:37
  93.3 12.7 %collective-permute-start.28 = (bf16[128,1024]{1,0:T(8,128)(2,1)S(1)}, bf16[128,1024]{1,0:T(8,128)(2,1)S(1)}, u32[]{:S(2)}, u32[]{:S(2)}) collective-permute-start(bf16[128,1024]{1,0:T(8,128)(2,1)S(1)} %get-tuple-element.49), channel_id=1, source_target_pairs={{0,12},{1,97},{2,14},{3,99},{4,0},{5,101},{6,2},{7,103},{8,4},{9,1... | collective-permute-start | bytes 786440 | tf_op jit(solution)/shard_map/ppermute | solution.py:37
  96.4 14.3 %collective-permute-start.29 = (bf16[128,1024]{1,0:T(8,128)(2,1)S(1)}, bf16[128,1024]{1,0:T(8,128)(2,1)S(1)}, u32[]{:S(2)}, u32[]{:S(2)}) collective-permute-start(bf16[128,1024]{1,0:T(8,128)(2,1)S(1)} %get-tuple-element.50), channel_id=1, source_target_pairs={{0,4},{1,33},{2,6},{3,35},{4,8},{5,37},{6,10},{7,39},{8,12},{9,41}... | collective-permute-start | bytes 786440 | tf_op jit(solution)/shard_map/ppermute | solution.py:37
  98.1 12.5 %collective-permute-start.30 = (bf16[128,1024]{1,0:T(8,128)(2,1)S(1)}, bf16[128,1024]{1,0:T(8,128)(2,1)S(1)}, u32[]{:S(2)}, u32[]{:S(2)}) collective-permute-start(bf16[128,1024]{1,0:T(8,128)(2,1)S(1)} %get-tuple-element.51), channel_id=1, source_target_pairs={{0,14},{1,113},{2,0},{3,115},{4,2},{5,117},{6,4},{7,119},{8,6},{9,... | collective-permute-start | bytes 786440 | tf_op jit(solution)/shard_map/ppermute | solution.py:37
  99.3 13.8 %collective-permute-start.31 = (bf16[128,1024]{1,0:T(8,128)(2,1)S(1)}, bf16[128,1024]{1,0:T(8,128)(2,1)S(1)}, u32[]{:S(2)}, u32[]{:S(2)}) collective-permute-start(bf16[128,1024]{1,0:T(8,128)(2,1)S(1)} %get-tuple-element.52), channel_id=1, source_target_pairs={{0,2},{1,17},{2,4},{3,19},{4,6},{5,21},{6,8},{7,23},{8,10},{9,25},... | collective-permute-start | bytes 786440 | tf_op jit(solution)/shard_map/ppermute | solution.py:37
  113.4 14.6 %collective-permute-start.32 = (bf16[64,1024]{1,0:T(8,128)(2,1)S(1)}, bf16[64,1024]{1,0:T(8,128)(2,1)S(1)}, u32[]{:S(2)}, u32[]{:S(2)}) collective-permute-start(bf16[64,1024]{1,0:T(8,128)(2,1)S(1)} %shard_map.93), channel_id=1, source_target_pairs={{0,64},{1,9},{2,66},{3,11},{4,68},{5,13},{6,70},{7,15},{8,72},{9,1... | collective-permute-start | bytes 393224 | tf_op jit(solution)/shard_map/ppermute | solution.py:37
  121.1 9.8 %collective-permute-start.33 = (bf16[64,1024]{1,0:T(8,128)(2,1)S(1)}, bf16[64,1024]{1,0:T(8,128)(2,1)S(1)}, u32[]{:S(2)}, u32[]{:S(2)}) collective-permute-start(bf16[64,1024]{1,0:T(8,128)(2,1)S(1)} %get-tuple-element.55), channel_id=1, source_target_pairs={{0,80},{1,11},{2,82},{3,13},{4,84},{5,15},{6,86},{7,1},{8,88},{9,3... | collective-permute-start | bytes 393224 | tf_op jit(solution)/shard_map/ppermute | solution.py:37
  121.3 9.7 %collective-permute-start.34 = (bf16[64,1024]{1,0:T(8,128)(2,1)S(1)}, bf16[64,1024]{1,0:T(8,128)(2,1)S(1)}, u32[]{:S(2)}, u32[]{:S(2)}) collective-permute-start(bf16[64,1024]{1,0:T(8,128)(2,1)S(1)} %get-tuple-element.56), channel_id=1, source_target_pairs={{0,48},{1,7},{2,50},{3,9},{4,52},{5,11},{6,54},{7,13},{8,56},{9,15... | collective-permute-start | bytes 393224 | tf_op jit(solution)/shard_map/ppermute | solution.py:37
  (16 other events, 101.2 us)
